TPU v7x, 256 devices: a whole 4x4x8 slice. The times are simulated.
256 devices in a mesh: sp: 32 (over z, x), fs: 4 (over y), tp: 2 (over core).
Axes of the slice: x: 4, y: 4, z: 8, core: 2. Of those that a mesh axis runs over, the one named last changes fastest.
Arguments:
- tokens: bfloat16 [4, 8192, 2048], P('fs', ('sp', 'tp')), may hold values from -6 to 6
- norm_gain: float32 [2048], replicated, may hold values from 0.1 to 1.9
- w_query: bfloat16 [2048, 1024], P('fs', 'tp'), may hold values from -0.125 to 0.125
- w_key: bfloat16 [2048, 1024], P('fs', 'tp'), may hold values from -0.125 to 0.125
- w_value: bfloat16 [2048, 1024], P('fs', 'tp'), may hold values from -0.125 to 0.125
- w_conv_value: bfloat16 [2048, 1024], P('fs', 'tp'), may hold values from -2 to 2
- w_conv_gate: bfloat16 [2048, 1024], P('fs', 'tp'), may hold values from -0.125 to 0.125
- key_offset: bfloat16 [8192, 16], P('sp', 'tp'), may hold values from -16 to 2
- conv_kernel: float32 [31, 1024], P(None, 'tp'), may hold values from -3 to 3
- conv_gain: float32 [1024], P('tp'), may hold values from 0.1 to 1.9
- w_attn_out: bfloat16 [1024, 2048], P('tp', 'fs'), may hold values from -1 to 1
- w_conv_out: bfloat16 [1024, 2048], P('tp', 'fs'), may hold values from -0.1875 to 0.1875
Outputs:
- mixed: bfloat16 [4, 8192, 2048], P('fs', ('sp', 'tp'))
All inputs are finite; a program needn't handle non-finite values.
Results may differ from a plain program's by a relative error of at most 0.0085.
Values may be sent and summed in bfloat16 or wider, within the bound.
A program may use at most 128 MiB of HBM per device.

v0:
```python
import jax
import jax.numpy as jnp
from jax import lax
from jax.sharding import PartitionSpec as P

HD = 64
CC = 1024


def sent_together(arrays, axis, dim, along):
    both = jnp.concatenate(arrays, axis=along)
    result, at, outs = (lax.all_gather(both, axis, axis=dim, tiled=True), 0, [])
    for a in arrays:
        outs.append(lax.slice_in_dim(result, at, at + a.shape[along], axis=along))
        at += a.shape[along]
    return tuple(outs)


def joined_along(parts, dim):
    lengths = list(parts.shape[1:])
    lengths[dim] *= parts.shape[0]
    return jnp.moveaxis(parts, 0, dim).reshape(lengths)


def copy_for_each(x, axis):
    copies = jnp.broadcast_to(x, (lax.axis_size(axis), *x.shape))
    return lax.all_to_all(copies, axis, split_axis=0, concat_axis=0, tiled=True)


def gather_directly(x, axis, dim):
    return joined_along(copy_for_each(x, axis), dim)


def shifted(block, axis, distance):
    devices = range(lax.axis_size(axis))
    route = [(i - distance, i) for i in devices if i - distance in devices]
    return lax.ppermute(block, axis, route)


def over_pieces(x, axis):
    return lax.all_gather(x, axis).sum(0)


def split_up(x, dim, size):
    before, after = (x.shape[:dim], x.shape[dim + 1 :])
    return jnp.moveaxis(x.reshape(*before, size, -1, *after), dim, 0)


def sum_at_owner(x, axis, dim):
    parts = split_up(x, dim, lax.axis_size(axis))
    arrived = lax.all_to_all(parts, axis, split_axis=0, concat_axis=0, tiled=True)
    return arrived.astype(jnp.float32).sum(axis=0)


def piece_terms(queries, key_rows, value_rows, offsets, carry_log, allowed):
    head_size = queries.shape[2]
    logits = jnp.einsum(
        "qhd,khd->hqk", queries, key_rows, preferred_element_type=jnp.float32
    ) * head_size ** (-0.5)
    logits = logits + jnp.transpose(offsets.astype(jnp.float32))[:, None, :]
    log_keep = jax.nn.log_sigmoid(-logits)
    if allowed is not None:
        log_keep = jnp.where(allowed[None], log_keep, 0.0)
    between = lax.cumsum(log_keep, axis=2, reverse=True) - log_keep
    weights = jnp.exp(jax.nn.log_sigmoid(logits) + between + carry_log[:, :, None])
    if allowed is not None:
        weights = jnp.where(allowed[None], weights, 0.0)
    result = jnp.einsum(
        "hqk,khd->qhd", weights.astype(jnp.bfloat16), value_rows, preferred_element_type=jnp.float32
    )
    return (result, carry_log + jnp.sum(log_keep, axis=2))


def shards(
    tokens,
    norm_gain,
    w_query,
    w_key,
    w_value,
    w_conv_value,
    w_conv_gate,
    key_offset,
    conv_kernel,
    conv_gain,
    w_attn_out,
    w_conv_out,
):
    gathered = sent_together((w_query, w_key, w_value, w_conv_value, w_conv_gate), "fs", 0, 1)
    floats = gather_directly(tokens[0], "tp", 0).astype(jnp.float32)
    normed = (
        floats * lax.rsqrt(jnp.mean(floats * floats, axis=1, keepdims=True) + 1e-06) * norm_gain
    ).astype(jnp.bfloat16)
    projected = jnp.concatenate(
        [
            jnp.dot(normed, weight, preferred_element_type=jnp.float32).astype(jnp.bfloat16)
            for weight in gathered
        ],
        axis=1,
    )
    head_cols = w_query.shape[1]
    channels = w_conv_value.shape[1]
    block_len = projected.shape[0]
    local_heads = head_cols // HD
    queries = projected[:, :head_cols].reshape(block_len, local_heads, HD)
    key_flat = projected[:, head_cols : 2 * head_cols]
    value_flat = projected[:, 2 * head_cols : 3 * head_cols]
    conv_value = projected[:, 3 * head_cols : 3 * head_cols + channels]
    conv_gate = projected[:, 3 * head_cols + channels :]
    position = lax.axis_index("sp")
    positions = jnp.arange(block_len, dtype=jnp.int32)
    causal = positions[None, :] < positions[:, None]
    start_log = jnp.zeros((local_heads, block_len), jnp.float32)
    totals, carry_log = piece_terms(
        queries,
        key_flat.reshape(block_len, local_heads, HD),
        value_flat.reshape(block_len, local_heads, HD),
        key_offset,
        start_log,
        causal,
    )
    all_keys, all_values, all_offsets = sent_together(
        (key_flat, value_flat, key_offset), "sp", 0, 1
    )

    def visit(hop_count, carried):
        running, running_log = carried
        source = (position - hop_count) * block_len
        piece_keys = lax.dynamic_slice_in_dim(all_keys, source, block_len, 0).reshape(
            block_len, local_heads, HD
        )
        piece_values = lax.dynamic_slice_in_dim(all_values, source, block_len, 0).reshape(
            block_len, local_heads, HD
        )
        piece_offsets = lax.dynamic_slice_in_dim(all_offsets, source, block_len, 0)
        result, next_log = piece_terms(
            queries, piece_keys, piece_values, piece_offsets, running_log, None
        )
        return (running + result, next_log)

    totals, carry_log = lax.fori_loop(1, position + 1, visit, (totals, carry_log))
    attn_heads = totals.reshape(block_len, head_cols).astype(jnp.bfloat16)
    gated_input = (
        conv_value.astype(jnp.float32) * jax.nn.sigmoid(conv_gate.astype(jnp.float32))
    ).astype(jnp.bfloat16)
    kernel_len = conv_kernel.shape[0]
    edge_rows = shifted(gated_input[block_len - (kernel_len - 1) :], "sp", 1)
    extended = jnp.concatenate([edge_rows, gated_input], axis=0).astype(jnp.float32)
    conv_sum = jnp.zeros((block_len, channels), jnp.float32)
    for tap_index in range(kernel_len):
        conv_sum = conv_sum + conv_kernel[tap_index] * extended[tap_index : tap_index + block_len]
    channel_total, channel_squares = (
        over_pieces(jnp.sum(conv_sum, axis=1), "tp"),
        over_pieces(jnp.sum(conv_sum * conv_sum, axis=1), "tp"),
    )
    mean_val = channel_total / CC
    centred = conv_sum - mean_val[:, None]
    spread = channel_squares / CC - mean_val * mean_val
    conv_hidden = jax.nn.silu(centred * lax.rsqrt(spread + 1e-06)[:, None] * conv_gain).astype(
        jnp.bfloat16
    )
    attn_weight, conv_weight = sent_together((w_attn_out, w_conv_out), "fs", 1, 0)
    partial_value = jnp.dot(attn_heads, attn_weight, preferred_element_type=jnp.float32)
    partial_value = partial_value + jnp.dot(
        conv_hidden, conv_weight, preferred_element_type=jnp.float32
    )
    mixed = sum_at_owner(
        lax.optimization_barrier(partial_value.astype(jnp.bfloat16))
        .astype(jnp.float32)
        .astype(jnp.bfloat16),
        "tp",
        0,
    )
    return mixed.astype(jnp.bfloat16)[None]


def solution(mesh):
    placed = (
        P("fs", ("sp", "tp"), None),
        P(),
        P("fs", "tp"),
        P("fs", "tp"),
        P("fs", "tp"),
        P("fs", "tp"),
        P("fs", "tp"),
        P("sp", "tp"),
        P(None, "tp"),
        P("tp"),
        P("tp", "fs"),
        P("tp", "fs"),
    )
    return jax.shard_map(
        shards, mesh=mesh, in_specs=placed, out_specs=P("fs", ("sp", "tp"), None), check_vma=False
    )
```

profile of v0, /device:TPU:231, one launch (start us, length us, event | category | flops | bytes accessed | tf_op | source)
XLA Modules:
  0.0 695.0 jit_solution(17368151743243712959)
XLA Ops:
  11.7 4.2 all-to-all-start
  18.3 95.9 %all-gather.8.cloned.1.call-done = bf16[2048,2560]{1,0:T(8,128)(2,1)} async-done(((bf16[512,2560]{1,0:T(8,128)(2,1)}), bf16[2048,2560]{1,0:T(8,128)(2,1)}) %all-gather.8.cloned.1.call-update) | async-done | bytes 10485776 | tf_op jit(solution)/shard_map/all_gather | solution.py:12
  132.5 5.1 fusion.36
  148.6 118.0 %all-gather.10.cloned.1.call-done = bf16[8192,1032]{1,0:T(8,128)(2,1)} async-done(((bf16[256,1032]{1,0:T(8,128)(2,1)}), bf16[8192,1032]{1,0:T(8,128)(2,1)}) %all-gather.10.cloned.1.call-update) | async-done | bytes 16908304 | tf_op jit(solution)/shard_map/all_gather | solution.py:12
  269.1 11.6 %fusion.117 = (bf16[8192,512]{1,0:T(8,128)(2,1)}, bf16[8192,512]{1,0:T(8,128)(2,1)}) fusion(bf16[8192,1032]{1,0:T(8,128)(2,1)} %all-gather.10.cloned.1.call-done), kind=kLoop, calls=%fused_computation.162 | loop fusion | bytes 33554432 | tf_op jit(solution)/shard_map/slice | solution.py:14
  280.7 397.4 %while.12 = (s32[]{:T(128)}, f32[256,8,64]{0,2,1:T(8,128)S(1)}, f32[8,256]{1,0:T(8,128)S(1)}, s32[]{:T(128)}, s32[]{:T(128)}, /*index=5*/bf16[8192,512]{1,0:T(8,...) while((s32[]{:T(128)}, f32[256,8,64]{0,2,1:T(8,128)S(1)}, ...), condition=%wide.region_8.9_spmd, body=%wide.region_4.8_spmd.sunk | while | flops 217720832 | bytes 27160768 | solution.py:140
  283.8 5.1 fusion.150
  289.8 3.2 fusion.152
  296.7 5.1 fusion.150
  302.6 3.2 fusion.152
  309.5 5.1 fusion.150
  315.5 3.2 fusion.152
  322.3 5.1 fusion.150
  328.3 3.2 fusion.152
  335.1 5.1 fusion.150
  341.1 3.2 fusion.152
  347.9 5.1 fusion.150
  353.9 3.2 fusion.152
  360.8 5.1 fusion.150
  366.7 3.2 fusion.152
  373.6 5.1 fusion.150
  379.6 3.2 fusion.152
  386.4 5.1 fusion.150
  392.4 3.2 fusion.152
  399.2 5.1 fusion.150
  405.2 3.2 fusion.152
  412.0 5.1 fusion.150
  418.0 3.2 fusion.152
  424.8 5.1 fusion.150
  430.8 3.2 fusion.152
  437.7 5.1 fusion.150
  443.6 3.2 fusion.152
  450.5 5.1 fusion.150
  456.5 3.2 fusion.152
  463.3 5.1 fusion.150
  469.3 3.2 fusion.152
  476.1 5.1 fusion.150
  482.1 3.2 fusion.152
  488.9 5.1 fusion.150
  494.9 3.2 fusion.152
  501.7 5.1 fusion.150
  507.7 3.2 fusion.152
  514.6 5.1 fusion.150
  520.5 3.2 fusion.152
  527.4 5.1 fusion.150
  533.4 3.2 fusion.152
  540.2 5.1 fusion.150
  546.2 3.2 fusion.152
  553.0 5.1 fusion.150
  565.8 5.1 fusion.150
  578.6 5.1 fusion.150
  591.5 5.1 fusion.150
  604.3 5.1 fusion.150
  610.3 3.2 fusion.152
  617.1 5.1 fusion.150
  623.1 3.2 fusion.152
  629.9 5.1 fusion.150
  635.9 3.2 fusion.152
  642.7 5.1 fusion.150
  648.7 3.2 fusion.152
  655.5 5.1 fusion.150
  661.5 3.2 fusion.152
  668.4 5.1 fusion.150
  681.8 5.6 all_to_all.10
  (426 shorter events, 196.5 us)
Async XLA Ops:
  6.5 2.3 copy-start.3
  6.5 107.7 %all-gather.8.cloned.1.call-start = ((), (), s32[]{:S(2)}) async-start(), calls=%async_computation.2 | async-start | bytes 13107200 | tf_op jit(solution)/shard_map/all_gather | solution.py:12
  6.5 2.3 copy-start.4
  6.5 2.4 copy-start.5
  8.9 1.6 copy-start.2
  9.0 1.5 copy-start
  10.5 5.4 copy-start.9
  10.5 7.4 %copy-start.10 = (f32[2048]{0:T(1024)S(1)}, f32[2048]{0:T(1024)}, u32[]{:S(2)}) copy-start(f32[2048]{0:T(1024)} %param.15) | copy-start | bytes 24580
  11.7 6.0 all-to-all-start
  15.9 250.7 %all-gather.10.cloned.1.call-start = ((), (), s32[]{:S(2)}) async-start(), calls=%async_computation.3 | async-start | bytes 19464192 | tf_op jit(solution)/shard_map/all_gather | solution.py:12
  116.5 3.4 copy-start.6
  116.5 3.4 copy-start.7
  119.8 1.2 copy-start.8
  119.9 558.3 %all-gather.12.cloned.1.call-start = ((), (), s32[]{:S(2)}) async-start(), calls=%async_computation.4 | async-start | bytes 5242880 | tf_op jit(solution)/shard_map/all_gather | solution.py:12
  126.1 15.5 %collective-permute-start = (bf16[30,512]{1,0:T(8,128)(2,1)S(1)}, bf16[30,512]{1,0:T(8,128)(2,1)S(1)}, u32[]{:S(2)}, u32[]{:S(2)}) collective-permute-start(bf16[30,512]{1,0:T(8,128)(2,1)S(1)} %slice.319), channel_id=1, source_target_pairs={{0,8},{8,16},{16,24},{24,32},{32,40},{40,48},{48,56},{56,64},{64,7... | collective-permute-start | bytes 92168 | tf_op jit(solution)/shard_map/ppermute | solution.py:37
  678.1 2.8 copy-start.1
  678.1 2.8 copy-start.11
Sparse Core Ops, SparseCore 0:
  10.6 103.5 all-gather.7
  120.0 146.5 all-gather.9
  268.4 52.2 all-gather.11
where the time goes:
time: 696 us; the launch traced here: 695 us
  other arithmetic  280 us (40%)
  waiting for transfers between devices  216 us (31%)
  matrix products  83.8 us (12%)
  local copies, waits for them, and re-layouts  83.2 us (12%)
  between operations  13.5 us (2%)
  blocking collectives  9.69 us (1%)
    all_gather x3, waiting for transfers between devices, sent_together(): result, at, outs = (lax.all_gather(both, axis, axis=dim, tiled=True), 0, [])  214 us
    another operation x64, other arithmetic  164 us
    convert_element_type x32, other arithmetic, piece_terms(): weights.astype(jnp.bfloat16)  103 us
    dot_general x32, matrix products, piece_terms(): jnp.einsum('qhd,khd->hqk', queries, key_rows, preferred_element_type=jnp....  59.1 us
    dynamic_slice x62, local copies, waits for them, and re-layouts, visit(): lax.dynamic_slice_in_dim(all_keys, source, block_len, 0)  37.3 us
    another operation x32, local copies, waits for them, and re-layouts, piece_terms(): between = lax.cumsum(log_keep, axis=2, reverse=True) - log_keep  21.7 us
  transfers between devices with their start and end apart: 5, of which 3 were waited for; matrix products, arithmetic and copies ran while one was open for 62% of the time, Pallas kernels for 0%

commit v1 on v0

v1 whole, which is shorter than its diff:
```python
import functools
import math

import jax
import jax.numpy as jnp
from jax import lax
from jax.experimental import pallas as pl
from jax.experimental.pallas import tpu as pltpu
from jax.sharding import Mesh
from jax.sharding import PartitionSpec as P

MESH = pl.DeviceIdType.MESH
F32 = jnp.float32
BF16 = jnp.bfloat16
LOG2E = math.log2(math.e)
TOP = 25.0
HD = 64
CC = 1024
KW = 31
UNIT = 1024
QB = 256
NZ = 8
NX = 4
EDGE = 32
VM = pl.BlockSpec(memory_space=pltpu.VMEM)
ANY = pl.BlockSpec(memory_space=pl.ANY)


def sems(*counts):
    return [pltpu.SemaphoreType.DMA((n,)) for n in counts]


def remote(src, dst, send, recv, **to):
    return pltpu.make_async_remote_copy(
        src_ref=src, dst_ref=dst, send_sem=send, recv_sem=recv, device_id=to, device_id_type=MESH
    )


def signal(**to):
    pl.semaphore_signal(
        pltpu.get_barrier_semaphore(), inc=1, device_id=to, device_id_type=MESH
    )


class Ring:
    def __init__(self, axis, me, at, send, recv):
        right, left = lax.rem(me + 1, 4), lax.rem(me + 3, 4)
        self.left, self.right = left, right

        def hop(block, half, slot, to):
            ref = at(block, half)
            return remote(ref, ref, send.at[slot], recv.at[slot], **{axis: to})

        self.first = [hop(me, 0, 0, right), hop(me, 1, 2, left), hop(me, 1, 1, right), hop(me, 0, 3, left)]
        self.second = [hop(left, 0, 4, right), hop(right, 1, 5, left)]

    def start(self):
        for copy in self.first:
            copy.start()

    def forward(self):
        for got, copy in zip(self.first[:2], self.second):
            got.wait_recv()
            copy.start()

    def neighbours(self):
        for copy in self.first[2:]:
            copy.wait_recv()

    def far(self):
        for copy in self.second:
            copy.wait_recv()

    def sent(self):
        for copy in self.first + self.second:
            copy.wait_send()


def collect_kernel(tok, gain, off, wq, wk, wv, wcv, wcg, rows, weights, offs, ws, xs, xr, ys, yr, ds, dr, os_, or_):
    x, y, c = (lax.axis_index(n) for n in ("x", "fs", "tp"))
    loads = [
        pltpu.make_async_copy(
            w.at[:, pl.ds(pl.multiple_of(x * 128, 128), 128)], weights.at[y, :, pl.ds(i * 128, 128)], ws.at[i]
        )
        for i, w in enumerate((wq, wk, wv, wcv, wcg))
    ]
    for load in loads:
        load.start()
    for d in (1, 2, 3):
        signal(x=lax.rem(x + d, 4))
    signal(fs=lax.rem(y + 1, 4))
    signal(fs=lax.rem(y + 3, 4))
    signal(tp=1 - c)

    def norm(i, _):
        at = pl.ds(pl.multiple_of(i * 16, 16), 16)
        floats = tok[at, :].astype(F32)
        scale = lax.rsqrt(jnp.mean(floats * floats, axis=1, keepdims=True) + 1e-06)
        rows[x, c, at, :] = (floats * scale * gain[...]).astype(BF16)
        return 0

    lax.fori_loop(0, 8, norm, 0)
    offs[x] = off[x]
    for load in loads:
        load.wait()
    pl.semaphore_wait(pltpu.get_barrier_semaphore(), 6)
    ring_y = Ring("fs", y, lambda b, h: weights.at[b, pl.ds(h * 256, 256)], ys, yr)
    ring_x = Ring("x", x, lambda b, h: rows.at[b, c, pl.ds(h * 64, 64)], xs, xr)

    def over(block, slot):
        ref = rows.at[block, c]
        return remote(ref, ref, ds.at[slot], dr.at[slot], tp=1 - c)

    across = [over(x, 0), over(ring_x.left, 1), over(ring_x.right, 2), over(lax.rem(x + 2, 4), 3)]
    ring_y.start()
    ring_x.start()
    across[0].start()
    small = [
        remote(off.at[lax.rem(x + d, 4)], offs.at[x], os_.at[d - 1], or_.at[d - 1], x=lax.rem(x + d, 4))
        for d in (1, 2, 3)
    ]
    for copy in small:
        copy.start()
    ring_x.forward()
    ring_y.forward()
    ring_x.neighbours()
    across[1].start()
    across[2].start()
    ring_x.far()
    across[3].start()
    for copy in small:
        copy.wait()
    ring_y.neighbours()
    ring_y.far()
    for copy in across:
        copy.wait()
    ring_x.sent()
    ring_y.sent()


def collect(tokens, gain, off, ws):
    return pl.pallas_call(
        collect_kernel,
        out_shape=(
            jax.ShapeDtypeStruct((NX, 2, 128, 2048), BF16),
            jax.ShapeDtypeStruct((4, 512, 640), BF16),
            jax.ShapeDtypeStruct((NX, 2, 8, 128), F32),
        ),
        in_specs=[VM, VM, VM] + [ANY] * 5,
        out_specs=(VM, VM, VM),
        scratch_shapes=sems(5, 6, 6, 6, 6, 4, 4, 3, 3),
        compiler_params=pltpu.CompilerParams(
            collective_id=1, has_side_effects=True, vmem_limit_bytes=40 * 2**20
        ),
        name="collect",
    )(tokens, gain, off, *ws)


def project_kernel(rows, weights, offs, qt, kp, vt, m, gated, kf, vf, vp):
    def block(b, _):
        at = pl.ds(pl.multiple_of(b * 256, 256), 256)
        total = None
        for f in range(4):
            part = jnp.dot(rows[at, pl.ds(f * 512, 512)], weights[f], preferred_element_type=F32)
            total = part if total is None else total + part
        kf[at, :] = total[:, 128:256]
        vf[at, :] = total[:, 256:384]
        q = total[:, :128].T
        qt[0, b] = q[:64].astype(BF16)
        qt[1, b] = q[64:].astype(BF16)
        value = total[:, 384:512].astype(BF16).astype(F32)
        gate = total[:, 512:640].astype(BF16).astype(F32)
        gated[at, :] = (value / (1.0 + jnp.exp(-gate))).astype(BF16)
        return 0

    lax.fori_loop(0, 4, block, 0)
    low = lax.broadcasted_iota(jnp.int32, (8, 128), 1) < 64

    def keys(i, _):
        ks = [[], []]
        for s in (0, 1):
            near = kf[pl.ds(2 * i + s, 8, stride=128), :]
            later = kf[pl.ds(2 * i + s + 64, 8, stride=128), :]
            ks[0].append(jnp.where(low, near, pltpu.roll(later, 64, 1)))
            ks[1].append(jnp.where(low, pltpu.roll(near, 64, 1), later))
        at = pl.ds(pl.multiple_of(i * 16, 16), 16)
        for j in (0, 1):
            kp[j, at, :] = jnp.concatenate(ks[j], axis=0).astype(BF16)
        return 0

    lax.fori_loop(0, 32, keys, 0, unroll=4)

    def values(i, _):
        vp[pl.ds(pl.multiple_of(i * 8, 8), 8), :] = vf[pl.ds(i, 8, stride=128), :]
        return 0

    lax.fori_loop(0, 128, values, 0, unroll=8)
    for b in range(8):
        v = vp[pl.ds(b * 128, 128), :].T.astype(BF16)
        vt[0, :, pl.ds(b * 128, 128)] = v[:64]
        vt[1, :, pl.ds(b * 128, 128)] = v[64:]
    sub = lax.broadcasted_iota(jnp.int32, (8, 128), 0)
    for j in (0, 1):
        tile = offs[0, j]
        for x in (1, 2, 3):
            tile = jnp.where(sub < 2 * x, tile, pltpu.roll(offs[x, j], 2 * x, 0))
        m[j] = tile


def project(rows, weights, offs):
    return pl.pallas_call(
        project_kernel,
        out_shape=(
            jax.ShapeDtypeStruct((2, 4, HD, QB), BF16),
            jax.ShapeDtypeStruct((2, 512, 128), BF16),
            jax.ShapeDtypeStruct((2, HD, UNIT), BF16),
            jax.ShapeDtypeStruct((2, 8, 128), F32),
            jax.ShapeDtypeStruct((UNIT, 128), BF16),
        ),
        in_specs=[VM] * 3,
        out_specs=(VM,) * 5,
        scratch_shapes=[pltpu.VMEM((UNIT, 128), F32)] * 3,
        compiler_params=pltpu.CompilerParams(vmem_limit_bytes=40 * 2**20),
        name="project",
    )(rows.reshape(UNIT, 2048), weights, offs)


def exchange_kernel(
    qt, kp, vt, m, gated, wa, wc, kin, vin, qin, min_, gin, wout,
    wl, ys, yr, zs, ks, vs, qs, ms, ds, dr, xs, xr, hs, hr,
):
    z, x, y, c = (lax.axis_index(n) for n in ("z", "x", "fs", "tp"))
    loads = [pltpu.make_async_copy(w, wout.at[y, i], wl.at[i]) for i, w in enumerate((wa, wc))]
    for load in loads:
        load.start()
    home = z // 4
    here = home == c
    order = [0, 1, 7, 2, 6, 3, 5, 4]
    for d in order:
        if d == 0:
            pl.when(jnp.logical_not(here))(lambda: signal(tp=1 - c))
        else:
            signal(z=lax.rem(z + d, 8), tp=home)
    signal(tp=1 - c)
    for d in (1, 2, 3):
        signal(x=lax.rem(x + d, 4))
    signal(fs=lax.rem(y + 1, 4))
    signal(fs=lax.rem(y + 3, 4))
    heir = jnp.logical_and(x == 0, z > 0)

    @pl.when(heir)
    def _():
        for s in range(4):
            signal(z=z - 1, x=s)

    @pl.when(jnp.logical_and(x == 0, z == 0))
    def _():
        for s in range(4):
            gin[s, pl.ds(0, EDGE), :] = jnp.zeros((EDGE, 128), BF16)

    for load in loads:
        load.wait()
    giver = z < 7
    pl.semaphore_wait(
        pltpu.get_barrier_semaphore(),
        14 - here.astype(jnp.int32) + giver.astype(jnp.int32),
    )

    sends = []

    def send(src, dst, slot, recv, zd, cd):
        same = jnp.logical_and(zd == z, cd == c)
        copy = remote(src, dst, zs.at[slot], recv, z=zd, tp=cd)

        @pl.when(same)
        def _():
            pltpu.make_async_copy(src, dst, recv).start()

        @pl.when(jnp.logical_not(same))
        def _():
            copy.start()

        sends.append((jnp.logical_not(same), copy))

    odd = lax.rem(z, 2)
    for jj in range(4):
        zd, j, half = 4 * c + jj, jj // 2, jj % 2
        send(kp.at[j], kin.at[z], 6 * jj, ks.at[z], zd, 0)
        send(vt.at[j], vin.at[z], 6 * jj + 1, vs.at[z], zd, 1)
        for cd in (0, 1):
            quarter = 2 * half + cd
            block = quarter + odd * (3 - 2 * quarter)
            send(qt.at[j, block], qin.at[z], 6 * jj + 2 + cd, qs.at[z], zd, cd)
            send(m.at[j], min_.at[z], 6 * jj + 4 + cd, ms.at[z], zd, cd)

    ring_y = Ring("fs", y, lambda b, h: wout.at[b, h], ys, yr)
    ring_y.start()

    def part(to):
        return gated.at[pl.ds(pl.multiple_of(to * 256 - EDGE, EDGE), 256 + EDGE), :]

    own = pltpu.make_async_copy
    rows_x = []
    for d in (1, 2, 3):
        to = lax.rem(x + d, 4)
        whole = remote(part(to), gin.at[x], xs.at[d - 1], xr.at[x], x=to)
        less = remote(
            gated.at[pl.ds(0, 256), :], gin.at[x, pl.ds(EDGE, 256), :], xs.at[d - 1], xr.at[x], x=to
        )
        pl.when(to > 0)(whole.start)
        pl.when(to == 0)(less.start)
        rows_x.append((to, whole, less))
    own_whole = own(part(x), gin.at[x], xr.at[x])
    own_less = own(gated.at[pl.ds(0, 256), :], gin.at[x, pl.ds(EDGE, 256), :], xr.at[x])
    pl.when(x > 0)(own_whole.start)
    pl.when(x == 0)(own_less.start)
    edge = remote(
        gated.at[pl.ds(UNIT - EDGE, EDGE), :], gin.at[x, pl.ds(0, EDGE), :], hs.at[0], hr.at[x], z=z + 1, x=0
    )
    pl.when(giver)(edge.start)

    def pass_on(at, source):
        ref, sem = (kin, ks) if at == 0 else (vin, vs)
        return remote(ref.at[source], ref.at[source], ds.at[source], sem.at[source], tp=1 - at)

    for core in (0, 1):
        @pl.when(c == core)
        def _(core=core):
            for n, d in enumerate(order):
                source = lax.rem(z + d, 8)
                copy = pass_on(core, source)
                copy.wait_recv()
                copy.start()
                if n == 4:
                    ring_y.forward()
            for d in order:
                source = lax.rem(z + d, 8)
                pass_on(1 - core, source).wait_recv()
                pass_on(core, source).wait_send()

    for d in order:
        source = lax.rem(z + d, 8)
        pltpu.make_async_copy(qt.at[0, 0], qin.at[source], qs.at[source]).wait()
        pltpu.make_async_copy(m.at[0], min_.at[source], ms.at[source]).wait()
    for s in range(4):
        pl.when(x > 0)(own(part(1), gin.at[s], xr.at[s]).wait)
        pl.when(x == 0)(own(gated.at[pl.ds(0, 256), :], gin.at[s, pl.ds(EDGE, 256), :], xr.at[s]).wait)
        pl.when(heir)(own(gated.at[pl.ds(0, EDGE), :], gin.at[s, pl.ds(0, EDGE), :], hr.at[s]).wait)
    for cond, copy in sends:
        pl.when(cond)(copy.wait_send)
    for to, whole, less in rows_x:
        pl.when(to > 0)(whole.wait_send)
        pl.when(to == 0)(less.wait_send)
    pl.when(giver)(edge.wait_send)
    ring_y.neighbours()
    ring_y.far()
    ring_y.sent()


def exchange(qt, kp, vt, m, gated, wa, wc):
    return pl.pallas_call(
        exchange_kernel,
        out_shape=(
            jax.ShapeDtypeStruct((NZ, 512, 128), BF16),
            jax.ShapeDtypeStruct((NZ, HD, UNIT), BF16),
            jax.ShapeDtypeStruct((NZ, HD, QB), BF16),
            jax.ShapeDtypeStruct((NZ, 8, 128), F32),
            jax.ShapeDtypeStruct((NX, 256 + EDGE, 128), BF16),
            jax.ShapeDtypeStruct((4, 2, 512, 512), BF16),
        ),
        in_specs=[VM] * 5 + [ANY] * 2,
        out_specs=(VM,) * 6,
        scratch_shapes=sems(2, 6, 6, 24, 8, 8, 8, 8, 8, 8, 3, 4, 1, 4),
        compiler_params=pltpu.CompilerParams(
            collective_id=2, has_side_effects=True, vmem_limit_bytes=40 * 2**20
        ),
        name="exchange",
    )(qt, kp, vt, m, gated, wa, wc)


def suffix(t):
    sub = lax.broadcasted_iota(jnp.int32, t.shape, 0)
    e = jnp.where(sub < 7, pltpu.roll(t, 7, 0), 1.0)
    for step in (1, 2, 4):
        e = e * jnp.where(sub < 8 - step, pltpu.roll(e, 8 - step, 0), 1.0)
    return e


def weigh(s_ref, cap, r_ref, w_ref, carry, first):
    t = None
    for g in range(31, -1, -1):
        d = []
        for j in range(4):
            rows = pl.ds((4 * g + j) * 8, 8)
            e = jnp.exp2(jnp.minimum(s_ref[rows, :] * LOG2E, cap[rows, :]))
            s_ref[rows, :] = e
            d.append(e + 1.0)
        r = 1.0 / ((d[0] * d[1]) * (d[2] * d[3]))
        r_ref[pl.ds(g * 8, 8), :] = r
        t = r if t is None else t * r
    start = jnp.where(first, 1.0, carry[...])
    p = suffix(t) * start
    carry[...] = jnp.broadcast_to((p * t)[0:1, :], p.shape)
    for g in range(31, -1, -1):
        e = [s_ref[pl.ds((4 * g + j) * 8, 8), :] for j in range(4)]
        p = p * r_ref[pl.ds(g * 8, 8), :]
        p1 = p * (e[0] + 1.0)
        p2 = p1 * (e[1] + 1.0)
        p3 = p2 * (e[2] + 1.0)
        w = jnp.concatenate([e[0] * p, e[1] * p1, e[2] * p2, e[3] * p3], axis=0)
        w_ref[pl.ds(g * 32, 32), :] = w.astype(BF16)


def attend_kernel(q_ref, k_ref, v_ref, m_ref, o_ref, qa, qb, off, s0, s1, w0, w1, r_ref, cap, carry, acc):
    z, c = lax.axis_index("z"), lax.axis_index("tp")
    quarter = 2 * lax.rem(z, 2) + c
    zero = jnp.zeros((HD, QB), BF16)
    row = lax.broadcasted_iota(jnp.int32, (128, QB), 0)
    one_a, one_b = ((row == i).astype(F32).astype(BF16) for i in (0, 1))

    def prepare(i, _):
        q = (q_ref[i].astype(F32) * 0.125).astype(BF16)
        qa[i] = jnp.concatenate([q, zero, one_a], axis=0)
        qb[i] = jnp.concatenate([zero, q, one_b], axis=0)
        tile = m_ref[i]
        col = lax.broadcasted_iota(jnp.int32, (8, 128), 1)
        for pair in range(32):
            both = []
            for n in (2 * pair, 2 * pair + 1):
                near = jnp.broadcast_to(tile[:, n : n + 1], (8, 128))
                later = jnp.broadcast_to(tile[:, n + 64 : n + 65], (8, 128))
                both.append(jnp.where(col == 0, near, jnp.where(col == 1, later, 0.0)))
            off[i, pl.ds(pair * 16, 16), :] = jnp.concatenate(both, axis=0).astype(BF16)
        return 0

    lax.fori_loop(0, NZ, prepare, 0)
    lane = lax.broadcasted_iota(jnp.int32, (8, QB), 1)
    sub = lax.broadcasted_iota(jnp.int32, (8, QB), 0)

    def caps(i, _):
        key = sub * 128 + i
        rows = pl.ds(pl.multiple_of(i * 8, 8), 8)
        cap[0, rows, :] = jnp.full((8, QB), TOP, F32)
        cap[1, rows, :] = jnp.where(key < lane + quarter * QB, TOP, -300.0)
        cap[2, rows, :] = jnp.where(key < lane + (3 - quarter) * QB, TOP, -300.0)
        return 0

    lax.fori_loop(0, 128, caps, 0, unroll=4)

    def following(u):
        zq, zk = u
        ends = zk == 0
        return (jnp.where(ends, zq + 1, zq), jnp.where(ends, zq + 1, zk - 1))

    def scores(u, s_ref):
        zq, zk = jnp.minimum(u[0], NZ - 1), jnp.minimum(u[1], NZ - 1)
        lhs = jnp.concatenate([k_ref[zk], off[zk]], axis=1)
        s_ref[0:512, :] = jnp.dot(lhs, qa[zq], preferred_element_type=F32)
        s_ref[512:1024, :] = jnp.dot(lhs, qb[zq], preferred_element_type=F32)

    def weights(u, s_ref, w_ref):
        zq, zk = u
        diagonal = zq == zk
        weigh(s_ref, cap.at[jnp.where(diagonal, 1 + lax.rem(zq, 2), 0)], r_ref, w_ref, carry, diagonal)

    def values(u, w_ref):
        zq, zk = u
        out = jnp.dot(v_ref[zk], w_ref[...], preferred_element_type=F32)
        acc[zq] = jnp.where(zq == zk, 0.0, acc[zq]) + out

    start = jnp.int32(0)
    carry[...] = jnp.ones_like(carry)
    w1[...] = jnp.zeros_like(w1)
    acc[0] = jnp.zeros_like(acc[0])
    scores((start, start), s0)

    def pair(_, state):
        before, now = state
        after = following(now)
        scores(after, s1)
        weights(now, s0, w0)
        values(before, w1)
        last = following(after)
        scores(last, s0)
        weights(after, s1, w1)
        values(now, w0)
        return (after, last)

    last, _ = lax.fori_loop(0, NZ * (NZ + 1) // 4, pair, ((start, start), (start, start)))
    values(last, w1)

    def finish(i, _):
        o_ref[i] = acc[i].astype(BF16)
        return 0

    lax.fori_loop(0, NZ, finish, 0)


def attend(q, k, v, m):
    return pl.pallas_call(
        attend_kernel,
        out_shape=jax.ShapeDtypeStruct((NZ, HD, QB), BF16),
        in_specs=[VM] * 4,
        out_specs=VM,
        scratch_shapes=[
            pltpu.VMEM((NZ, 256, QB), BF16),
            pltpu.VMEM((NZ, 256, QB), BF16),
            pltpu.VMEM((NZ, 512, 128), BF16),
            pltpu.VMEM((UNIT, QB), F32),
            pltpu.VMEM((UNIT, QB), F32),
            pltpu.VMEM((UNIT, QB), BF16),
            pltpu.VMEM((UNIT, QB), BF16),
            pltpu.VMEM((256, QB), F32),
            pltpu.VMEM((3, UNIT, QB), F32),
            pltpu.VMEM((8, QB), F32),
            pltpu.VMEM((NZ, HD, QB), F32),
        ],
        compiler_params=pltpu.CompilerParams(vmem_limit_bytes=48 * 2**20),
        name="attend",
    )(q, k, v, m)


def hand_back_kernel(o, oin, ss, rs):
    z, x, c = (lax.axis_index(n) for n in ("z", "x", "tp"))
    home = z // 4
    quarter = 2 * lax.rem(z, 2) + c
    head = 2 * x + lax.rem(z // 2, 2)
    wanted = x + lax.rem(z, 2) * (3 - 2 * x)
    for h in range(8):
        zs, xs, cs = 4 * c + 2 * (h % 2) + wanted // 2, h // 2, lax.rem(wanted, 2)
        self_ = jnp.logical_and(jnp.logical_and(zs == z, xs == x), cs == c)
        pl.when(jnp.logical_not(self_))(lambda zs=zs, xs=xs, cs=cs: signal(z=zs, x=xs, tp=cs))
    copies = []
    mine = jnp.int32(0)
    for zq in range(NZ):
        xd = quarter if zq % 2 == 0 else 3 - quarter
        self_ = jnp.logical_and(jnp.logical_and(z == zq, xd == x), home == c)
        mine = mine + self_.astype(jnp.int32)
        copies.append(
            (self_, remote(o.at[zq], oin.at[head], ss.at[zq], rs.at[head], z=zq, x=xd, tp=home), zq)
        )
    pl.semaphore_wait(pltpu.get_barrier_semaphore(), 8 - mine)
    for self_, copy, zq in copies:
        pl.when(jnp.logical_not(self_))(copy.start)
        pl.when(self_)(pltpu.make_async_copy(o.at[zq], oin.at[head], rs.at[head]).start)
    for h in range(8):
        pltpu.make_async_copy(o.at[0], oin.at[h], rs.at[h]).wait()
    for self_, copy, zq in copies:
        pl.when(jnp.logical_not(self_))(copy.wait_send)


def hand_back(o):
    return pl.pallas_call(
        hand_back_kernel,
        out_shape=jax.ShapeDtypeStruct((8, HD, QB), BF16),
        in_specs=[VM],
        out_specs=VM,
        scratch_shapes=sems(8, 8),
        compiler_params=pltpu.CompilerParams(collective_id=3, has_side_effects=True),
        name="hand_back",
    )(o)


def shards(
    tokens, norm_gain, w_query, w_key, w_value, w_conv_value, w_conv_gate,
    key_offset, conv_kernel, conv_gain, w_attn_out, w_conv_out,
):
    tile = key_offset.astype(F32).T.reshape(NX, 2, 2, 128)
    tile = jnp.pad(tile, ((0, 0), (0, 0), (0, 6), (0, 0)))
    rows, weights, offs = collect(
        tokens[0], norm_gain[None], tile, (w_query, w_key, w_value, w_conv_value, w_conv_gate)
    )
    qt, kp, vt, m, gated = project(rows, weights, offs)
    kin, vin, qin, min_, gin, wout = exchange(qt, kp, vt, m, gated, w_attn_out, w_conv_out)
    o = attend(qin, kin, vin, min_)
    heads = hand_back(o).reshape(512, QB)

    extended = jnp.moveaxis(gin, 0, 1).reshape(256 + EDGE, 512).astype(F32)
    conv_sum = jnp.zeros((256, 512), F32)
    for tap in range(KW):
        at = EDGE - (KW - 1) + tap
        conv_sum = conv_sum + conv_kernel[tap] * extended[at : at + 256]
    sums = jnp.stack([jnp.sum(conv_sum, axis=1), jnp.sum(conv_sum * conv_sum, axis=1)])
    sums = lax.all_gather(sums, "tp").sum(0)
    mean = sums[0] / CC
    spread = sums[1] / CC - mean * mean
    hidden = jax.nn.silu(
        (conv_sum - mean[:, None]) * lax.rsqrt(spread + 1e-06)[:, None] * conv_gain
    ).astype(BF16)

    wo = jnp.moveaxis(wout, 0, 2).reshape(2, 512, 2048)
    partial = lax.dot_general(heads, wo[0], (((0,), (0,)), ((), ())), preferred_element_type=F32)
    partial = partial + jnp.dot(hidden, wo[1], preferred_element_type=F32)
    parts = lax.optimization_barrier(partial.astype(BF16)).reshape(2, 128, 2048)
    arrived = lax.all_to_all(parts, "tp", split_axis=0, concat_axis=0, tiled=True)
    return arrived.astype(F32).sum(axis=0).astype(BF16)[None]


def solution(mesh):
    view = Mesh(mesh.devices.reshape(NZ, NX, 4, 2), ("z", "x", "fs", "tp"))
    rows = P("fs", ("z", "x", "tp"), None)
    placed = (
        rows, P(), P("fs", "tp"), P("fs", "tp"), P("fs", "tp"), P("fs", "tp"), P("fs", "tp"),
        P(("z", "x"), "tp"), P(None, "tp"), P("tp"), P("tp", "fs"), P("tp", "fs"),
    )
    return jax.shard_map(shards, mesh=view, in_specs=placed, out_specs=rows, check_vma=False)
```

time: 696 us -> 226 us (0.32)
  the two profiles are of different devices: /device:TPU:231 before, /device:TPU:1 now
where the time goes in v1:
time: 226 us; the launch traced here: 223 us
  Pallas kernels  116 us (51%)
  local copies, waits for them, and re-layouts  89.7 us (40%)
  other arithmetic  8.77 us (4%)
  blocking collectives  6.34 us (3%)
    slice x35, local copies, waits for them, and re-layouts, shards(): conv_sum = conv_sum + conv_kernel[tap] * extended[at:at + 256]  69.4 us
    pallas_call x1, Pallas kernels, exchange(): pl.pallas_call(exchange_kernel, out_shape=(jax.ShapeDtypeStruct((NZ, 512,...  43.1 us
    pallas_call x1, Pallas kernels, collect(): pl.pallas_call(collect_kernel, out_shape=(jax.ShapeDtypeStruct((NX, 2, 12...  28 us
    pallas_call x1, Pallas kernels, hand_back(): pl.pallas_call(hand_back_kernel, out_shape=jax.ShapeDtypeStruct((8, HD, Q...  20 us
    pallas_call x1, Pallas kernels, attend(): pl.pallas_call(attend_kernel, out_shape=jax.ShapeDtypeStruct((NZ, HD, QB)...  19.8 us
    unnamed x32, local copies, waits for them, and re-layouts  10.5 us
    reduce_sum x1, other arithmetic, shards(): jnp.sum(conv_sum, axis=1)  7.57 us
    slice x2, local copies, waits for them, and re-layouts, shards(): partial = partial + jnp.dot(hidden, wo[1], preferred_element_type=F32)  6.2 us

profile of v1, /device:TPU:1, one launch (start us, length us, event | category | flops | bytes accessed | tf_op | source)
XLA Modules:
  0.0 223.0 jit_solution(5985916871232941544)
XLA Ops:
  0.0 1.0 fusion.42
  1.0 1.2 fusion.41
  2.2 0.7 reshape.73
  2.9 1.0 copy-done.2
  3.9 1.0 copy-done.3
  5.0 1.0 copy-done.4
  6.0 1.0 copy-done.5
  7.1 1.0 copy-done.6
  8.1 1.0 copy-done.7
  9.1 0.7 copy-done.10
  9.8 28.0 %collect.1 = (bf16[4,2,128,2048]{3,2,1,0:T(8,128)(2,1)S(1)}, bf16[4,512,640]{2,1,0:T(8,128)(2,1)S(1)}, f32[4,2,8,128]{3,2,1,0:T(8,128)S(1)}) custom-call(bf16[128,2048]{1,0:T(8,128)(2,1)S(1)} %bitcast.267, f32[1,2048]{1,0:T(1,128)S(1)} %bitcast.268, f32[4,2,8,128]{3,2,1,0:T(8,128)S(1)} %pad_convert_fusion.off, bf16[512,512]{1,0:T(8,128)(2,1)S(1)} %copy-done.3, ...), custom_call_target="tpu_custom_call" | custom-call | tf_op jit(solution)/shard_map/collect/pallas_call | solution.py:142
  37.9 0.0 copy-start.8
  37.9 0.0 copy-start.9
  37.9 5.4 %project.1 = (bf16[2,4,64,256]{3,2,1,0:T(8,128)(2,1)S(1)}, bf16[2,512,128]{2,1,0:T(8,128)(2,1)S(1)}, bf16[2,64,1024]{2,1,0:T(8,128)(2,1)S(1)}, f32[2,8,128]{2,1,0:T(8,128)S(1)}, bf16[1024,128]{1,0:T(8,128)(2,1)S(1)}) custom-call(bf16[1024,2048]{1,0:T(8,128)(2,1)S(1)} %bitcast.266, bf16[4,512,640]{2,1,0:T(8,128)(2,1)S(1)} %get-tuple-element.20.weights, ...), custom_call_target="tpu_custom_call" | custom-call | tf_op jit(solution)/shard_map/project/pallas_call | solution.py:211
  43.3 43.1 %exchange.1 = (bf16[8,512,128]{2,1,0:T(8,128)(2,1)S(1)}, bf16[8,64,1024]{2,1,0:T(8,128)(2,1)S(1)}, bf16[8,64,256]{2,1,0:T(8,128)(2,1)S(1)}, f32[8,8,128]{2,1,0:T...) custom-call(bf16[2,4,64,256]{3,2,1,0:T(8,128)(2,1)S(1)} %get-tuple-element.22.qt, ...), custom_call_target="tpu_custom_call" | custom-call | tf_op jit(solution)/shard_map/exchange/pallas_call | solution.py:361
  86.4 1.9 copy-done
  88.4 2.6 %fusion.40 = (f32[256,4,128]{2,0,1:T(8,128)}, f32[256,4,128]{2,0,1:T(8,128)}, f32[256,4,128]{2,0,1:T(8,128)}, f32[256,4,128]{2,0,1:T(8,128)}, f32[256,4,128]{2,0...) fusion(f32[288,4,128]{2,0,1:T(8,128)S(1)} %convert_bitcast_fusion), kind=kLoop, calls=%fused_computation.79 | loop fusion | bytes 12582912 | tf_op jit(solution)/shard_map/slice | solution.py:582
  91.0 3.8 %fusion.39 = (f32[256,4,128]{2,0,1:T(8,128)}, f32[256,4,128]{2,0,1:T(8,128)}, f32[256,4,128]{2,0,1:T(8,128)}, f32[256,4,128]{2,0,1:T(8,128)}, f32[256,4,128]{2,0...) fusion(f32[288,4,128]{2,0,1:T(8,128)S(1)} %convert_bitcast_fusion), kind=kLoop, calls=%fused_computation.78 | loop fusion | bytes 19922944 | tf_op jit(solution)/shard_map/slice | solution.py:582
  94.9 19.8 %attend.1.o = bf16[8,64,256]{2,1,0:T(8,128)(2,1)S(1)} custom-call(bf16[8,64,256]{2,1,0:T(8,128)(2,1)S(1)} %get-tuple-element.27.q_ref, bf16[8,512,128]{2,1,0:T(8,128)(2,1)S(1)} %get-tuple-element.28.k_ref, bf16[8,64,1024]{2,1,0:T(8,128)(2,1)S(1)} %get-tuple-element.29.v_ref, f32[8,8,128]{2,1,0:T(8,128)S(1)} %get-tuple-element.30.m_ref), custom_call_target="tpu_custom_call" | custom-call | tf_op jit(solution)/shard_map/attend/pallas_call | solution.py:500
  114.7 0.7 copy-done.1
  115.4 20.0 %hand_back.1 = bf16[8,64,256]{2,1,0:T(8,128)(2,1)} custom-call(bf16[8,64,256]{2,1,0:T(8,128)(2,1)} %copy-done.1), custom_call_target="tpu_custom_call" | custom-call | tf_op jit(solution)/shard_map/hand_back/pallas_call | solution.py:553
  135.4 3.8 %fusion.38 = (bf16[1,512,4,512]{3,1,0,2:T(8,128)(2,1)S(1)}, bf16[1,512,4,512]{3,1,0,2:T(8,128)(2,1)}) fusion(bf16[2,512,4,512]{3,1,0,2:T(8,128)(2,1)} %bitcast.265), kind=kLoop, calls=%fused_computation.77 | loop fusion | bytes 8388608 | tf_op jit(solution)/shard_map/slice | solution.py:593
  139.2 2.4 %copy.78 = bf16[1,512,4,512]{1,3,2,0:T(8,128)(2,1)} copy(bf16[1,512,4,512]{3,1,0,2:T(8,128)(2,1)S(1)} %get-tuple-element.36) | data formatting | bytes 4194304 | tf_op jit(solution)/shard_map/slice | solution.py:593
  141.6 2.8 %copy.46 = bf16[1,512,4,512]{1,3,2,0:T(8,128)(2,1)S(1)} copy(bf16[1,512,4,512]{3,1,0,2:T(8,128)(2,1)} %get-tuple-element.37) | data formatting | bytes 4194304 | tf_op jit(solution)/shard_map/slice | solution.py:592
  144.4 0.2 copy.48
  144.6 1.2 copy.59
  145.9 2.0 copy.58
  147.9 2.0 copy.57
  150.0 2.0 copy.56
  152.0 2.0 copy.55
  154.0 2.0 copy.54
  156.1 2.0 copy.53
  158.1 2.1 copy.52
  160.2 2.1 copy.51
  162.3 2.1 copy.50
  164.3 2.0 copy.49
  166.4 2.0 copy.47
  168.4 2.0 copy.77
  170.4 2.1 copy.76
  172.5 2.0 copy.75
  174.6 2.0 copy.74
  176.6 2.1 copy.73
  178.6 2.1 copy.72
  180.7 2.1 copy.71
  182.8 2.0 copy.70
  184.8 2.0 copy.69
  186.8 2.0 copy.68
  188.9 2.0 copy.67
  190.9 2.0 copy.66
  192.9 2.0 copy.65
  195.0 2.1 copy.64
  197.1 2.1 copy.63
  199.1 2.1 copy.62
  201.2 2.0 copy.61
  203.2 2.0 copy.60
  205.3 7.6 %fusion.36 = (f32[256]{0:T(256)S(1)}, f32[256]{0:T(256)S(1)}, f32[256,512]{0,1:T(8,128)}) fusion(f32[256,4,128]{0,2,1:T(8,128)} %copy.77, f32[512]{0:T(512)S(1)} %bitcast.283, f32[256,4,128]{0,2,1:T(8,128)} %copy.76, f32[512]{0:T(512)S(1)} %bitcast.284, f32[256,4,128]{0,2,1:T(8,128)} %copy.75, f32[512]{0:T(512)S(1)} %bitcast.286, f32[256,4,128]{0,2,1:T(8,128)} %copy.74, ...), kind=kLoop, calls=%fused_computation.76 | loop fusion | flops 8388096 | bytes 16842752 | tf_op jit(solution)/shard_map/reduce_sum | solution.py:583
  212.9 1.8 all-gather.1
  214.8 0.0 copy-start.15
  214.8 0.8 fusion.43
  215.5 0.8 copy-done.12
  216.3 0.1 copy-done.14
  216.4 0.9 fusion
  217.4 4.5 %all_to_all.5 = bf16[2,128,2048]{2,1,0:T(8,128)(2,1)S(1)} all-to-all(bf16[2,128,2048]{2,1,0:T(8,128)(2,1)S(1)} %bitcast.272), channel_id=1, replica_groups=mesh['z'=8,'x'=4,'fs'=4,'tp'=2] {'tp'}, dimensions={0} | all-to-all | bytes 2097152 | tf_op jit(solution)/shard_map/all_to_all | solution.py:595
  221.9 1.1 reduce_sum.42
  (24 shorter events, 0.1 us)
Async XLA Ops:
  2.9 1.0 copy-start.2
  3.9 1.0 copy-start.3
  5.0 1.0 copy-start.4
  6.0 1.0 copy-start.5
  7.1 1.0 copy-start.6
  8.1 1.0 copy-start.7
  9.1 0.7 copy-start.10
  37.9 5.4 %copy-start.8 = (bf16[512,512]{1,0:T(8,128)(2,1)S(1)}, bf16[512,512]{1,0:T(8,128)(2,1)}, u32[]{:S(2)}) copy-start(bf16[512,512]{1,0:T(8,128)(2,1)} %wa.1) | copy-start | bytes 1572868
  37.9 5.4 %copy-start.9 = (bf16[512,512]{1,0:T(8,128)(2,1)S(1)}, bf16[512,512]{1,0:T(8,128)(2,1)}, u32[]{:S(2)}) copy-start(bf16[512,512]{1,0:T(8,128)(2,1)} %wc.1) | copy-start | bytes 1572868
  86.4 1.9 copy-start
  114.7 0.7 copy-start.1
  141.6 2.9 %copy-start.11 = (f32[256,4,128]{2,0,1:T(8,128)S(1)}, f32[256,4,128]{2,0,1:T(8,128)}, u32[]{:S(2)}) copy-start(f32[256,4,128]{2,0,1:T(8,128)} %get-tuple-element.57) | copy-start | bytes 1572868
  205.3 9.5 %copy-start.13 = (bf16[8,64,256]{2,1,0:T(8,128)(2,1)S(1)}, bf16[8,64,256]{2,1,0:T(8,128)(2,1)}, u32[]{:S(2)}) copy-start(bf16[8,64,256]{2,1,0:T(8,128)(2,1)} %hand_back.1) | copy-start | bytes 786436
  214.7 1.6 copy-start.12
  214.7 1.7 copy-start.14
  214.8 1.7 copy-start.15

commit v2 on v1

v2 whole, which is shorter than its diff:
```python
import functools
import math

import jax
import jax.numpy as jnp
from jax import lax
from jax.experimental import pallas as pl
from jax.experimental.pallas import tpu as pltpu
from jax.sharding import Mesh
from jax.sharding import PartitionSpec as P

MESH = pl.DeviceIdType.MESH
F32 = jnp.float32
BF16 = jnp.bfloat16
LOG2E = math.log2(math.e)
TOP = 25.0
HD = 64
CC = 1024
KW = 31
UNIT = 1024
QB = 256
NZ = 8
NX = 4
EDGE = 32
VM = pl.BlockSpec(memory_space=pltpu.VMEM)
HBM = pl.BlockSpec(memory_space=pltpu.HBM)


def sems(*counts):
    return [pltpu.SemaphoreType.DMA((n,)) for n in counts]


def remote(src, dst, send, recv, **to):
    return pltpu.make_async_remote_copy(
        src_ref=src, dst_ref=dst, send_sem=send, recv_sem=recv, device_id=to, device_id_type=MESH
    )


def signal(**to):
    pl.semaphore_signal(
        pltpu.get_barrier_semaphore(), inc=1, device_id=to, device_id_type=MESH
    )


class Ring:
    def __init__(self, axis, me, at, send, recv):
        right, left = lax.rem(me + 1, 4), lax.rem(me + 3, 4)
        self.left, self.right = left, right

        def hop(block, half, slot, to):
            ref = at(block, half)
            return remote(ref, ref, send.at[slot], recv.at[slot], **{axis: to})

        self.first = [hop(me, 0, 0, right), hop(me, 1, 2, left), hop(me, 1, 1, right), hop(me, 0, 3, left)]
        self.second = [hop(left, 0, 4, right), hop(right, 1, 5, left)]

    def start(self):
        for copy in self.first:
            copy.start()

    def forward(self):
        for got, copy in zip(self.first[:2], self.second):
            got.wait_recv()
            copy.start()

    def neighbours(self):
        for copy in self.first[2:]:
            copy.wait_recv()

    def far(self):
        for copy in self.second:
            copy.wait_recv()

    def sent(self):
        for copy in self.first + self.second:
            copy.wait_send()


def suffix(t):
    sub = lax.broadcasted_iota(jnp.int32, t.shape, 0)
    e = jnp.where(sub < 7, pltpu.roll(t, 7, 0), 1.0)
    for step in (1, 2, 4):
        e = e * jnp.where(sub < 8 - step, pltpu.roll(e, 8 - step, 0), 1.0)
    return e


def weigh(s_ref, cap, r_ref, w_ref, left):
    t = None
    for g in range(31, -1, -1):
        d = []
        for j in range(4):
            rows = pl.ds((4 * g + j) * 8, 8)
            e = jnp.exp2(jnp.minimum(s_ref[rows, :] * LOG2E, cap[rows, :]))
            s_ref[rows, :] = e
            d.append(e + 1.0)
        r = 1.0 / ((d[0] * d[1]) * (d[2] * d[3]))
        r_ref[pl.ds(g * 8, 8), :] = r
        t = r if t is None else t * r
    p = suffix(t)
    left[...] = jnp.broadcast_to((p * t)[0:1, :], p.shape)
    for g in range(31, -1, -1):
        e = [s_ref[pl.ds((4 * g + j) * 8, 8), :] for j in range(4)]
        p = p * r_ref[pl.ds(g * 8, 8), :]
        p1 = p * (e[0] + 1.0)
        p2 = p1 * (e[1] + 1.0)
        p3 = p2 * (e[2] + 1.0)
        w = jnp.concatenate([e[0] * p, e[1] * p1, e[2] * p2, e[3] * p3], axis=0)
        w_ref[pl.ds(g * 32, 32), :] = w.astype(BF16)


def nth(n):
    half = n // 2
    return jnp.where(lax.rem(n, 2) == 1, 4 - half, lax.rem(8 - half, 8))


def layer_kernel(
    tok, tok_gain, offx, taps, gain, wq, wk, wv, wcv, wcg, wa, wc, out_ref,
    rows, weights, offs, full, kf, vf, vp, qt, kp, vt, m, gated,
    kin, vin, qin, min_, gin, wout, ext, csum, stat, stat_in, hidden, heads, own_part, part_out, part_in,
    qa, qb, off, s0, s1, w0, w1, r_ref, cap, left, acc, oout, oin,
    ws, cxs, cxr, cys, cyr, cds, cdr, cos, cor,
    wl, ys, yr, zs, ks, vs, qs, ms, ds, dr, xs, xr, hs, hr, ss, sr, os_, or_, ps, pr,
):
    z, x, y, c = (lax.axis_index(n) for n in ("z", "x", "fs", "tp"))
    first_loads = [
        pltpu.make_async_copy(
            w.at[:, pl.ds(pl.multiple_of(x * 128, 128), 128)], weights.at[y, :, pl.ds(i * 128, 128)], ws.at[i]
        )
        for i, w in enumerate((wq, wk, wv, wcv, wcg))
    ]
    loads = [pltpu.make_async_copy(w, wout.at[y, i], wl.at[i]) for i, w in enumerate((wa, wc))]
    for load in first_loads + loads:
        load.start()
    home = z // 4
    here = home == c
    other = jnp.logical_not
    local = pltpu.make_async_copy
    for d in range(8):
        if d == 0:
            pl.when(other(here))(lambda: signal(tp=1 - c))
        else:
            signal(z=lax.rem(z + d, 8), tp=home)
    signal(tp=1 - c)
    for d in (1, 2, 3):
        signal(x=lax.rem(x + d, 4))
    signal(fs=lax.rem(y + 1, 4))
    signal(fs=lax.rem(y + 3, 4))
    first_x = x == 0
    heir = jnp.logical_and(first_x, z > 0)
    giver = z < 7

    @pl.when(heir)
    def _():
        for s in range(4):
            signal(z=z - 1, x=s)

    quarter = 2 * lax.rem(z, 2) + c
    head = 2 * x + lax.rem(z // 2, 2)
    wanted = x + lax.rem(z, 2) * (3 - 2 * x)
    for h in range(8):
        zh, xh, ch = 4 * c + 2 * (h % 2) + wanted // 2, h // 2, lax.rem(wanted, 2)
        self_ = jnp.logical_and(jnp.logical_and(zh == z, xh == x), ch == c)
        pl.when(other(self_))(lambda zh=zh, xh=xh, ch=ch: signal(z=zh, x=xh, tp=ch))
    backs = []
    mine = jnp.int32(0)
    for zq in range(NZ):
        xd = quarter if zq % 2 == 0 else 3 - quarter
        self_ = jnp.logical_and(jnp.logical_and(z == zq, xd == x), here)
        mine = mine + self_.astype(jnp.int32)
        copy = remote(oout.at[zq], oin.at[head], os_.at[zq], or_.at[head], z=zq, x=xd, tp=home)
        backs.append((self_, copy, zq))

    def norm(i, _):
        at = pl.ds(pl.multiple_of(i * 16, 16), 16)
        floats = tok[at, :].astype(F32)
        scale = lax.rsqrt(jnp.mean(floats * floats, axis=1, keepdims=True) + 1e-06)
        rows[x, c, at, :] = (floats * scale * tok_gain[...]).astype(BF16)
        return 0

    lax.fori_loop(0, 8, norm, 0)
    offs[x] = offx[x]
    for load in first_loads:
        load.wait()
    pl.semaphore_wait(
        pltpu.get_barrier_semaphore(),
        22 - here.astype(jnp.int32) + giver.astype(jnp.int32) - mine,
    )

    ring_w = Ring("fs", y, lambda b, h: weights.at[b, pl.ds(h * 256, 256)], cys, cyr)
    ring_x = Ring("x", x, lambda b, h: rows.at[b, c, pl.ds(h * 64, 64)], cxs, cxr)

    def over(block, slot):
        ref = rows.at[block, c]
        return remote(ref, ref, cds.at[slot], cdr.at[slot], tp=1 - c)

    across = [over(x, 0), over(ring_x.left, 1), over(ring_x.right, 2), over(lax.rem(x + 2, 4), 3)]
    ring_w.start()
    ring_x.start()
    across[0].start()
    small = [
        remote(offx.at[lax.rem(x + d, 4)], offs.at[x], cos.at[d - 1], cor.at[d - 1], x=lax.rem(x + d, 4))
        for d in (1, 2, 3)
    ]
    for copy in small:
        copy.start()
    lane = lax.broadcasted_iota(jnp.int32, (8, QB), 1)
    sub = lax.broadcasted_iota(jnp.int32, (8, QB), 0)

    def caps(i, _):
        key = sub * 128 + i
        rows = pl.ds(pl.multiple_of(i * 8, 8), 8)
        cap[0, rows, :] = jnp.full((8, QB), TOP, F32)
        cap[1, rows, :] = jnp.where(key < lane + quarter * QB, TOP, -300.0)
        cap[2, rows, :] = jnp.where(key < lane + (3 - quarter) * QB, TOP, -300.0)
        return 0

    lax.fori_loop(0, 128, caps, 0, unroll=4)
    ring_x.forward()
    ring_w.forward()
    ring_x.neighbours()
    across[1].start()
    across[2].start()
    ring_x.far()
    across[3].start()
    for copy in small:
        copy.wait()
    for load in loads:
        load.wait()
    for copy in across:
        copy.wait()
    ring_w.neighbours()

    def near(b, _):
        at = pl.ds(pl.multiple_of(b * 256, 256), 256)
        total = None
        for f in (y, ring_w.left, ring_w.right):
            cols = pl.ds(pl.multiple_of(f * 512, 512), 512)
            lhs = jnp.concatenate([rows[b, 0, :, cols], rows[b, 1, :, cols]], axis=0)
            part = jnp.dot(lhs, weights[f], preferred_element_type=F32)
            total = part if total is None else total + part
        full[at, :] = total
        return 0

    lax.fori_loop(0, 4, near, 0)
    ring_w.far()
    far = lax.rem(y + 2, 4)

    def block(b, _):
        at = pl.ds(pl.multiple_of(b * 256, 256), 256)
        cols = pl.ds(pl.multiple_of(far * 512, 512), 512)
        lhs = jnp.concatenate([rows[b, 0, :, cols], rows[b, 1, :, cols]], axis=0)
        total = full[at, :] + jnp.dot(lhs, weights[far], preferred_element_type=F32)
        kf[at, :] = total[:, 128:256]
        vf[at, :] = total[:, 256:384]
        q = total[:, :128].T
        qt[0, b] = q[:64].astype(BF16)
        qt[1, b] = q[64:].astype(BF16)
        value = total[:, 384:512].astype(BF16).astype(F32)
        gate = total[:, 512:640].astype(BF16).astype(F32)
        gated[at, :] = (value / (1.0 + jnp.exp(-gate))).astype(BF16)
        return 0

    lax.fori_loop(0, 4, block, 0)
    low = lax.broadcasted_iota(jnp.int32, (8, 128), 1) < 64

    def keys(i, _):
        packed = [[], []]
        for s in (0, 1):
            near_ = kf[pl.ds(2 * i + s, 8, stride=128), :]
            later = kf[pl.ds(2 * i + s + 64, 8, stride=128), :]
            packed[0].append(jnp.where(low, near_, pltpu.roll(later, 64, 1)))
            packed[1].append(jnp.where(low, pltpu.roll(near_, 64, 1), later))
        at = pl.ds(pl.multiple_of(i * 16, 16), 16)
        for j in (0, 1):
            kp[j, at, :] = jnp.concatenate(packed[j], axis=0).astype(BF16)
        return 0

    lax.fori_loop(0, 32, keys, 0, unroll=4)

    def ordered(i, _):
        vp[pl.ds(pl.multiple_of(i * 8, 8), 8), :] = vf[pl.ds(i, 8, stride=128), :]
        return 0

    lax.fori_loop(0, 128, ordered, 0, unroll=8)
    for b in range(8):
        v = vp[pl.ds(b * 128, 128), :].T.astype(BF16)
        vt[0, :, pl.ds(b * 128, 128)] = v[:64]
        vt[1, :, pl.ds(b * 128, 128)] = v[64:]
    sub_ = lax.broadcasted_iota(jnp.int32, (8, 128), 0)
    for j in (0, 1):
        tile = offs[0, j]
        for s in (1, 2, 3):
            tile = jnp.where(sub_ < 2 * s, tile, pltpu.roll(offs[s, j], 2 * s, 0))
        m[j] = tile

    sends = []

    def send(src, dst, slot, recv, zd, cd):
        same = jnp.logical_and(zd == z, cd == c)
        copy = remote(src, dst, zs.at[slot], recv, z=zd, tp=cd)
        pl.when(same)(local(src, dst, recv).start)
        pl.when(other(same))(copy.start)
        sends.append((other(same), copy))

    odd = lax.rem(z, 2)
    for e in range(4):
        jj = lax.rem(z + e, 4)
        zd, j, half = 4 * c + jj, jj // 2, lax.rem(jj, 2)
        for cd in (0, 1):
            q4 = 2 * half + cd
            send(qt.at[j, q4 + odd * (3 - 2 * q4)], qin.at[z], 6 * e + 2 + cd, qs.at[z], zd, cd)
            send(m.at[j], min_.at[z], 6 * e + 4 + cd, ms.at[z], zd, cd)
        send(kp.at[j], kin.at[z], 6 * e, ks.at[z], zd, 0)
        send(vt.at[j], vin.at[z], 6 * e + 1, vs.at[z], zd, 1)

    short = gated.at[pl.ds(0, 256), :]
    edge_rows = pl.ds(0, EDGE)

    def part(to):
        return gated.at[pl.ds(pl.multiple_of(to * 256 - EDGE, EDGE), 256 + EDGE), :]

    rows_x = []
    for d in (1, 2, 3):
        to = lax.rem(x + d, 4)
        whole = remote(part(to), gin.at[x], xs.at[d - 1], xr.at[x], x=to)
        less = remote(short, gin.at[x, pl.ds(EDGE, 256), :], xs.at[d - 1], xr.at[x], x=to)
        pl.when(to > 0)(whole.start)
        pl.when(to == 0)(less.start)
        rows_x.append((to, whole, less))
    pl.when(other(first_x))(local(part(x), gin.at[x], xr.at[x]).start)
    pl.when(first_x)(local(short, gin.at[x, pl.ds(EDGE, 256), :], xr.at[x]).start)
    edge = remote(
        gated.at[pl.ds(UNIT - EDGE, EDGE), :], gin.at[x, edge_rows, :], hs.at[0], hr.at[x], z=z + 1, x=0
    )
    pl.when(giver)(edge.start)
    ring_y = Ring("fs", y, lambda b, h: wout.at[b, h], ys, yr)
    ring_y.start()

    @pl.when(jnp.logical_and(first_x, z == 0))
    def _():
        for s in range(4):
            gin[s, edge_rows, :] = jnp.zeros((EDGE, 128), BF16)

    for s in range(4):
        pl.when(other(first_x))(local(part(1), gin.at[s], xr.at[s]).wait)
        pl.when(first_x)(local(short, gin.at[s, pl.ds(EDGE, 256), :], xr.at[s]).wait)
        pl.when(heir)(local(gated.at[edge_rows, :], gin.at[s, edge_rows, :], hr.at[s]).wait)
    for s in range(4):
        ext[s] = gin[s].astype(F32)
    for s in range(4):
        cols = pl.ds(s * 128, 128)

        def block(i, _, s=s, cols=cols):
            at = pl.multiple_of(i * 32, 32)
            total = jnp.zeros((32, 128), F32)
            for tap in range(KW):
                total = total + taps[pl.ds(tap, 1), cols] * ext[s, pl.ds(at + EDGE - (KW - 1) + tap, 32), :]
            rows = pl.ds(at, 32)
            csum[rows, cols] = total
            square = total * total
            if s > 0:
                total = total + stat[0, rows, :]
                square = square + stat[1, rows, :]
            if s == 3:
                total = jnp.broadcast_to(jnp.sum(total, axis=1, keepdims=True), (32, 128))
                square = jnp.broadcast_to(jnp.sum(square, axis=1, keepdims=True), (32, 128))
            stat[0, rows, :] = total
            stat[1, rows, :] = square
            return 0

        lax.fori_loop(0, 8, block, 0)

    zero = jnp.zeros((HD, QB), BF16)
    row = lax.broadcasted_iota(jnp.int32, (128, QB), 0)
    one_a, one_b = ((row == i).astype(F32).astype(BF16) for i in (0, 1))
    col = lax.broadcasted_iota(jnp.int32, (8, 128), 1)

    def pass_on(at, source):
        ref, sem = (kin, ks) if at == 0 else (vin, vs)
        return remote(ref.at[source], ref.at[source], ds.at[source], sem.at[source], tp=1 - at)

    def arrive(n):
        source = lax.rem(z + nth(n), 8)
        for core in (0, 1):
            @pl.when(c == core)
            def _(core=core):
                copy = pass_on(core, source)
                copy.wait_recv()
                copy.start()

        pl.when(n == 3)(ring_y.forward)
        local(qt.at[0, 0], qin.at[source], qs.at[source]).wait()
        local(m.at[0], min_.at[source], ms.at[source]).wait()
        q = (qin[source].astype(F32) * 0.125).astype(BF16)
        qa[source] = jnp.concatenate([q, zero, one_a], axis=0)
        qb[source] = jnp.concatenate([zero, q, one_b], axis=0)
        tile = min_[source]
        for i in range(32):
            both = []
            for k in (2 * i, 2 * i + 1):
                near = jnp.broadcast_to(tile[:, k : k + 1], (8, 128))
                later = jnp.broadcast_to(tile[:, k + 64 : k + 65], (8, 128))
                both.append(jnp.where(col == 0, near, jnp.where(col == 1, later, 0.0)))
            off[source, pl.ds(i * 16, 16), :] = jnp.concatenate(both, axis=0).astype(BF16)
        for core in (0, 1):
            pl.when(c == core)(lambda core=core: pass_on(1 - core, source).wait_recv())

    def where_is(u):
        one, two = lax.rem(z + nth(u[0]), 8), lax.rem(z + nth(u[1]), 8)
        return jnp.maximum(one, two), jnp.minimum(one, two)

    def following(u):
        n, k = u
        ends = k == n
        return (jnp.where(ends, n + 1, n), jnp.where(ends, 0, k + 1))

    def scores(u, s_ref):
        pl.when(jnp.logical_and(u[1] == 0, u[0] < NZ))(lambda: arrive(u[0]))
        zq, zk = where_is((jnp.minimum(u[0], NZ - 1), u[1]))
        lhs = jnp.concatenate([kin[zk], off[zk]], axis=1)
        s_ref[0:512, :] = jnp.dot(lhs, qa[zq], preferred_element_type=F32)
        s_ref[512:1024, :] = jnp.dot(lhs, qb[zq], preferred_element_type=F32)

    def weights(u, s_ref, w_ref):
        zq, zk = where_is(u)
        which = jnp.where(zq == zk, 1 + lax.rem(zq, 2), 0)
        weigh(s_ref, cap.at[which], r_ref, w_ref, left.at[zq * NZ + zk])

    def values(u, w_ref):
        zq, zk = where_is(u)
        acc[zq * NZ + zk] = jnp.dot(vin[zk], w_ref[...], preferred_element_type=F32)

    start = jnp.int32(0)
    w1[...] = jnp.zeros_like(w1)
    scores((start, start), s0)

    remote(stat, stat_in, ss.at[0], sr.at[0], tp=1 - c).start()

    def pair(_, state):
        before, now = state
        after = following(now)
        scores(after, s1)
        weights(now, s0, w0)
        values(before, w1)
        last = following(after)
        scores(last, s0)
        weights(after, s1, w1)
        values(now, w0)
        return (after, last)

    last, _ = lax.fori_loop(0, NZ * (NZ + 1) // 4, pair, ((start, start), (start, start)))
    values(last, w1)

    for zq in range(NZ):
        total = acc[zq * NZ + zq].reshape(8, 8, QB)
        rest = left[zq * NZ + zq]
        for zk in range(zq - 1, -1, -1):
            total = total + acc[zq * NZ + zk].reshape(8, 8, QB) * rest[None]
            if zk > 0:
                rest = rest * left[zq * NZ + zk]
        oout[zq] = total.reshape(HD, QB).astype(BF16)
    for self_, copy, zq in backs:
        pl.when(other(self_))(copy.start)
        pl.when(self_)(local(oout.at[zq], oin.at[head], or_.at[head]).start)

    remote(stat, stat_in, ss.at[0], sr.at[0], tp=1 - c).wait()

    def finish(i, _):
        rows = pl.ds(pl.multiple_of(i * 32, 32), 32)
        mean = (stat[0, rows, :] + stat_in[0, rows, :]) / CC
        spread = (stat[1, rows, :] + stat_in[1, rows, :]) / CC - mean * mean
        scale = lax.rsqrt(spread + 1e-06)
        for s in range(4):
            cols = pl.ds(s * 128, 128)
            h = (csum[rows, cols] - mean) * scale * gain[:, cols]
            hidden[rows, cols] = (h / (1.0 + jnp.exp(-h))).astype(BF16)
        return 0

    lax.fori_loop(0, 8, finish, 0)
    ring_y.neighbours()
    ring_y.far()
    for h in range(8):
        local(oout.at[0], oin.at[h], or_.at[h]).wait()
    heads[...] = oin[...].reshape(512, QB).astype(F32).T.astype(BF16)
    theirs = []
    for f in range(4):
        total = jnp.dot(heads[...], wout[f, 0], preferred_element_type=F32)
        total = (total + jnp.dot(hidden[...], wout[f, 1], preferred_element_type=F32)).astype(BF16)
        low, high = total[:128], total[128:]
        own_part[f] = jnp.where(c == 0, low, high)
        part_out[f] = jnp.where(c == 0, high, low)
        theirs.append(remote(part_out.at[f], part_in.at[f], ps.at[f], pr.at[f], tp=1 - c))
    for copy in theirs:
        copy.start()
    for f, copy in enumerate(theirs):
        copy.wait()
        total = own_part[f].astype(F32) + part_in[f].astype(F32)
        out_ref[:, pl.ds(f * 512, 512)] = total.astype(BF16)

    for cond, copy in sends:
        pl.when(cond)(copy.wait_send)
    for to, whole, less in rows_x:
        pl.when(to > 0)(whole.wait_send)
        pl.when(to == 0)(less.wait_send)
    pl.when(giver)(edge.wait_send)
    for self_, copy, zq in backs:
        pl.when(other(self_))(copy.wait_send)
    for core in (0, 1):
        @pl.when(c == core)
        def _(core=core):
            for source in range(NZ):
                pass_on(core, source).wait_send()

    ring_y.sent()
    ring_x.sent()
    ring_w.sent()


def layer(tokens, tok_gain, offx, taps, gain, *ws):
    vm = pltpu.VMEM
    return pl.pallas_call(
        layer_kernel,
        out_shape=jax.ShapeDtypeStruct((128, 2048), BF16),
        in_specs=[VM] * 5 + [HBM] * 7,
        out_specs=VM,
        scratch_shapes=[
            vm((NX, 2, 128, 2048), BF16),
            vm((4, 512, 640), BF16),
            vm((NX, 2, 8, 128), F32),
            vm((UNIT, 640), F32),
            vm((UNIT, 128), F32),
            vm((UNIT, 128), F32),
            vm((UNIT, 128), F32),
            vm((2, 4, HD, QB), BF16),
            vm((2, 512, 128), BF16),
            vm((2, HD, UNIT), BF16),
            vm((2, 8, 128), F32),
            vm((UNIT, 128), BF16),
            vm((NZ, 512, 128), BF16),
            vm((NZ, HD, UNIT), BF16),
            vm((NZ, HD, QB), BF16),
            vm((NZ, 8, 128), F32),
            vm((NX, 256 + EDGE, 128), BF16),
            vm((4, 2, 512, 512), BF16),
            vm((NX, 256 + EDGE, 128), F32),
            vm((256, 512), F32),
            vm((2, 256, 128), F32),
            vm((2, 256, 128), F32),
            vm((256, 512), BF16),
            vm((256, 512), BF16),
            vm((4, 128, 512), BF16),
            vm((4, 128, 512), BF16),
            vm((4, 128, 512), BF16),
            vm((NZ, 256, QB), BF16),
            vm((NZ, 256, QB), BF16),
            vm((NZ, 512, 128), BF16),
            vm((UNIT, QB), F32),
            vm((UNIT, QB), F32),
            vm((UNIT, QB), BF16),
            vm((UNIT, QB), BF16),
            vm((256, QB), F32),
            vm((3, UNIT, QB), F32),
            vm((NZ * NZ, 8, QB), F32),
            vm((NZ * NZ, HD, QB), F32),
            vm((NZ, HD, QB), BF16),
            vm((8, HD, QB), BF16),
        ]
        + sems(5, 6, 6, 6, 6, 4, 4, 3, 3)
        + sems(2, 6, 6, 24, 8, 8, 8, 8, 8, 8, 3, 4, 1, 4, 1, 1, 8, 8, 4, 4),
        compiler_params=pltpu.CompilerParams(
            collective_id=1, has_side_effects=True, vmem_limit_bytes=63 * 2**20
        ),
        name="layer",
    )(tokens, tok_gain, offx, taps, gain, *ws)


def shards(
    tokens, norm_gain, w_query, w_key, w_value, w_conv_value, w_conv_gate,
    key_offset, conv_kernel, conv_gain, w_attn_out, w_conv_out,
):
    tile = key_offset.astype(F32).T.reshape(NX, 2, 2, 128)
    tile = jnp.pad(tile, ((0, 0), (0, 0), (0, 6), (0, 0)))
    return layer(
        tokens[0], norm_gain[None], tile, conv_kernel, conv_gain[None],
        w_query, w_key, w_value, w_conv_value, w_conv_gate, w_attn_out, w_conv_out,
    )[None]


def solution(mesh):
    view = Mesh(mesh.devices.reshape(NZ, NX, 4, 2), ("z", "x", "fs", "tp"))
    rows = P("fs", ("z", "x", "tp"), None)
    placed = (
        rows, P(), P("fs", "tp"), P("fs", "tp"), P("fs", "tp"), P("fs", "tp"), P("fs", "tp"),
        P(("z", "x"), "tp"), P(None, "tp"), P("tp"), P("tp", "fs"), P("tp", "fs"),
    )
    return jax.shard_map(shards, mesh=view, in_specs=placed, out_specs=rows, check_vma=False)
```

time: 226 us -> 121 us (0.54); the launches traced: 223 us -> 120 us
  local copies, waits for them, and re-layouts: 89.7 us -> 2.58 us
  other arithmetic: 8.77 us -> 0.62 us
  blocking collectives: 6.34 us -> 0 us
    slice x38 -> x0, local copies, waits for them, and re-layouts: 78.5 us -> none  [the longest x35 69.4 us: shards(): conv_sum = conv_sum + conv_kernel[tap] * extended[at:at + 256]]
    reduce_sum x3 -> x0, other arithmetic: 8.7 us -> none  [the longest x1 7.57 us: shards(): jnp.sum(conv_sum, axis=1)]
    unnamed x32 -> x3, local copies, waits for them, and re-layouts: 10.5 us -> 2.57 us
    all_to_all x1 -> x0, blocking collectives: 4.5 us -> none  [shards(): lax.all_to_all(parts, 'tp', split_axis=0, concat_axis=0, tiled=True)]
    pallas_call x5 -> x1, Pallas kernels: 116 us -> 117 us  [layer(): pl.pallas_call(layer_kernel, out_shape=jax.ShapeDtypeStruct((128, 2048),...]
where the time goes in v2:
time: 121 us; the launch traced here: 120 us
  Pallas kernels  117 us (97%)
  local copies, waits for them, and re-layouts  2.58 us (2%)
    pallas_call x1, Pallas kernels, layer(): pl.pallas_call(layer_kernel, out_shape=jax.ShapeDtypeStruct((128, 2048),...  117 us
    unnamed x3, local copies, waits for them, and re-layouts  2.57 us

profile of v2, /device:TPU:1, one launch (start us, length us, event | category | flops | bytes accessed | tf_op | source)
XLA Modules:
  0.0 120.4 jit_solution(12343756541227418423)
XLA Ops:
  0.0 0.0 copy-start
  0.0 0.7 copy-done
  0.7 0.6 pad_convert_fusion.offx
  1.3 117.1 %layer.1 = bf16[128,2048]{1,0:T(8,128)(2,1)} custom-call(bf16[128,2048]{1,0:T(8,128)(2,1)} %bitcast.6, f32[1,2048]{1,0:T(1,128)} %bitcast.7, f32[4,2,8,128]{3,2,1,0:T(8,128)} %pad_convert_fusion.offx, f32[31,512]{1,0:T(8,128)} %taps.1, f32[1,512]{1,0:T(1,128)} %bitcast.9, bf16[512,512]{1,0:T(8,128)(2,1)} %wq.1, bf16[512,512]{1,0:T(8,128)(2,1)} %wk.1, ...), custom_call_target="tpu_custom_call" | custom-call | tf_op jit(solution)/shard_map/layer/pallas_call | solution.py:521
  118.5 1.9 %copy.14 = bf16[1,128,2048]{2,1,0:T(8,128)(2,1)} copy(bf16[1,128,2048]{2,1,0:T(8,128)(2,1)} %bitcast.5) | data formatting | bytes 1048576
  (1 shorter events, 0.0 us)
Async XLA Ops:
  0.0 0.7 copy-start

commit v3 on v2

--- a/solution.py
+++ b/solution.py
@@ -84,42 +84,52 @@
     return e
 
 
-def weigh(s_ref, cap, r_ref, w_ref, left):
+def keep(score, cap, e_ref, r_ref, t_ref):
     t = None
-    for g in range(31, -1, -1):
+    for g in [n // 2 + 16 * (n % 2) for n in range(32)]:
         d = []
         for j in range(4):
-            rows = pl.ds((4 * g + j) * 8, 8)
-            e = jnp.exp2(jnp.minimum(s_ref[rows, :] * LOG2E, cap[rows, :]))
-            s_ref[rows, :] = e
+            i = 4 * g + j
+            rows = pl.ds(i * 8, 8)
+            e = jnp.exp2(jnp.minimum(score[i * 8 : i * 8 + 8], cap[rows, :]))
+            e_ref[rows, :] = e
             d.append(e + 1.0)
         r = 1.0 / ((d[0] * d[1]) * (d[2] * d[3]))
         r_ref[pl.ds(g * 8, 8), :] = r
         t = r if t is None else t * r
+    t_ref[...] = t
+
+
+def weigh(e_ref, r_ref, t_ref, w_ref, left):
+    t = t_ref[...]
     p = suffix(t)
     left[...] = jnp.broadcast_to((p * t)[0:1, :], p.shape)
     for g in range(31, -1, -1):
-        e = [s_ref[pl.ds((4 * g + j) * 8, 8), :] for j in range(4)]
         p = p * r_ref[pl.ds(g * 8, 8), :]
-        p1 = p * (e[0] + 1.0)
-        p2 = p1 * (e[1] + 1.0)
-        p3 = p2 * (e[2] + 1.0)
-        w = jnp.concatenate([e[0] * p, e[1] * p1, e[2] * p2, e[3] * p3], axis=0)
-        w_ref[pl.ds(g * 32, 32), :] = w.astype(BF16)
+        rest, w = p, []
+        for j in range(4):
+            w.append(e_ref[pl.ds((4 * g + j) * 8, 8), :] * rest)
+            rest = rest + w[j]
+        w_ref[pl.ds(g * 32, 32), :] = jnp.concatenate(w, axis=0).astype(BF16)
+
+
+ARRIVAL = (0, 7, 3, 1, 5, 6, 2, 4)
 
 
 def nth(n):
-    half = n // 2
-    return jnp.where(lax.rem(n, 2) == 1, 4 - half, lax.rem(8 - half, 8))
+    d = jnp.int32(ARRIVAL[0])
+    for k in range(1, NZ):
+        d = jnp.where(n == k, ARRIVAL[k], d)
+    return d
 
 
 def layer_kernel(
     tok, tok_gain, offx, taps, gain, wq, wk, wv, wcv, wcg, wa, wc, out_ref,
     rows, weights, offs, full, kf, vf, vp, qt, kp, vt, m, gated,
     kin, vin, qin, min_, gin, wout, ext, csum, stat, stat_in, hidden, heads, own_part, part_out, part_in,
-    qa, qb, off, s0, s1, w0, w1, r_ref, cap, left, acc, oout, oin,
+    qa, keys_in, e0, e1, w0, w1, r0, r1, t0, t1, cap, left, acc, oout, oin,
     ws, cxs, cxr, cys, cyr, cds, cdr, cos, cor,
-    wl, ys, yr, zs, ks, vs, qs, ms, ds, dr, xs, xr, hs, hr, ss, sr, os_, or_, ps, pr,
+    wl, ys, yr, zs, ks, vs, qs, ms, ds, fs, xs, xr, hs, hr, ss, sr, os_, or_, ps, pr,
 ):
     z, x, y, c = (lax.axis_index(n) for n in ("z", "x", "fs", "tp"))
     first_loads = [
@@ -140,7 +150,9 @@
             pl.when(other(here))(lambda: signal(tp=1 - c))
         else:
             signal(z=lax.rem(z + d, 8), tp=home)
+    partner = z + 1 - 2 * lax.rem(z, 2)
     signal(tp=1 - c)
+    signal(z=partner)
     for d in (1, 2, 3):
         signal(x=lax.rem(x + d, 4))
     signal(fs=lax.rem(y + 1, 4))
@@ -183,7 +195,7 @@
         load.wait()
     pl.semaphore_wait(
         pltpu.get_barrier_semaphore(),
-        22 - here.astype(jnp.int32) + giver.astype(jnp.int32) - mine,
+        23 - here.astype(jnp.int32) + giver.astype(jnp.int32) - mine,
     )
 
     ring_w = Ring("fs", y, lambda b, h: weights.at[b, pl.ds(h * 256, 256)], cys, cyr)
@@ -220,17 +232,11 @@
     ring_x.neighbours()
     across[1].start()
     across[2].start()
-    ring_x.far()
-    across[3].start()
-    for copy in small:
-        copy.wait()
     for load in loads:
         load.wait()
-    for copy in across:
-        copy.wait()
     ring_w.neighbours()
 
-    def near(b, _):
+    def near(b):
         at = pl.ds(pl.multiple_of(b * 256, 256), 256)
         total = None
         for f in (y, ring_w.left, ring_w.right):
@@ -239,9 +245,19 @@
             part = jnp.dot(lhs, weights[f], preferred_element_type=F32)
             total = part if total is None else total + part
         full[at, :] = total
-        return 0
-
-    lax.fori_loop(0, 4, near, 0)
+
+    across[0].wait()
+    near(x)
+    across[1].wait()
+    near(ring_x.left)
+    ring_x.far()
+    across[3].start()
+    across[2].wait()
+    near(ring_x.right)
+    for copy in small:
+        copy.wait()
+    across[3].wait()
+    near(lax.rem(x + 2, 4))
     ring_w.far()
     far = lax.rem(y + 2, 4)
 
@@ -295,24 +311,16 @@
 
     sends = []
 
-    def send(src, dst, slot, recv, zd, cd):
+    def send(src, dst, slot, recv, zd, cd, cond=None):
         same = jnp.logical_and(zd == z, cd == c)
+        away = other(same) if cond is None else jnp.logical_and(other(same), cond)
+        near_ = same if cond is None else jnp.logical_and(same, cond)
         copy = remote(src, dst, zs.at[slot], recv, z=zd, tp=cd)
-        pl.when(same)(local(src, dst, recv).start)
-        pl.when(other(same))(copy.start)
-        sends.append((other(same), copy))
+        pl.when(near_)(local(src, dst, recv).start)
+        pl.when(away)(copy.start)
+        sends.append((away, copy))
 
     odd = lax.rem(z, 2)
-    for e in range(4):
-        jj = lax.rem(z + e, 4)
-        zd, j, half = 4 * c + jj, jj // 2, lax.rem(jj, 2)
-        for cd in (0, 1):
-            q4 = 2 * half + cd
-            send(qt.at[j, q4 + odd * (3 - 2 * q4)], qin.at[z], 6 * e + 2 + cd, qs.at[z], zd, cd)
-            send(m.at[j], min_.at[z], 6 * e + 4 + cd, ms.at[z], zd, cd)
-        send(kp.at[j], kin.at[z], 6 * e, ks.at[z], zd, 0)
-        send(vt.at[j], vin.at[z], 6 * e + 1, vs.at[z], zd, 1)
-
     short = gated.at[pl.ds(0, 256), :]
     edge_rows = pl.ds(0, EDGE)
 
@@ -333,6 +341,15 @@
         gated.at[pl.ds(UNIT - EDGE, EDGE), :], gin.at[x, edge_rows, :], hs.at[0], hr.at[x], z=z + 1, x=0
     )
     pl.when(giver)(edge.start)
+    for e in (0, 1, 3, 2):
+        jj = lax.rem(z + e, 4)
+        zd, j, half = 4 * c + jj, jj // 2, lax.rem(jj, 2)
+        for cd in (0, 1):
+            q4 = 2 * half + cd
+            send(qt.at[j, q4 + odd * (3 - 2 * q4)], qin.at[z], 6 * e + 2 + cd, qs.at[z], zd, cd)
+            send(m.at[j], min_.at[z], 6 * e + 4 + cd, ms.at[z], zd, cd)
+        send(kp.at[j], kin.at[z], 6 * e, ks.at[z], zd, 0, here if e == 0 else None)
+        send(vt.at[j], vin.at[z], 6 * e + 1, vs.at[z], zd, 1, here if e == 0 else None)
     ring_y = Ring("fs", y, lambda b, h: wout.at[b, h], ys, yr)
     ring_y.start()
 
@@ -371,39 +388,54 @@
         lax.fori_loop(0, 8, block, 0)
 
     zero = jnp.zeros((HD, QB), BF16)
-    row = lax.broadcasted_iota(jnp.int32, (128, QB), 0)
-    one_a, one_b = ((row == i).astype(F32).astype(BF16) for i in (0, 1))
+    ones = (lax.broadcasted_iota(jnp.int32, (HD, QB), 0) < 2).astype(F32).astype(BF16)
     col = lax.broadcasted_iota(jnp.int32, (8, 128), 1)
 
     def pass_on(at, source):
         ref, sem = (kin, ks) if at == 0 else (vin, vs)
         return remote(ref.at[source], ref.at[source], ds.at[source], sem.at[source], tp=1 - at)
 
-    def arrive(n):
+    opposite = lax.rem(partner + 4, 8)
+
+    def hand_on(at):
+        ref, sem = (kin, ks) if at == 0 else (vin, vs)
+        return remote(ref.at[opposite], ref.at[opposite], fs.at[0], sem.at[opposite], z=partner)
+
+    def share(n):
         source = lax.rem(z + nth(n), 8)
         for core in (0, 1):
             @pl.when(c == core)
             def _(core=core):
                 copy = pass_on(core, source)
                 copy.wait_recv()
+                pl.when(source == opposite)(hand_on(core).start)
                 copy.start()
 
+    def arrive(n):
+        source = lax.rem(z + nth(n), 8)
+        pl.when(n < NZ - 1)(lambda: share(n + 1))
         pl.when(n == 3)(ring_y.forward)
         local(qt.at[0, 0], qin.at[source], qs.at[source]).wait()
         local(m.at[0], min_.at[source], ms.at[source]).wait()
-        q = (qin[source].astype(F32) * 0.125).astype(BF16)
-        qa[source] = jnp.concatenate([q, zero, one_a], axis=0)
-        qb[source] = jnp.concatenate([zero, q, one_b], axis=0)
-        tile = min_[source]
-        for i in range(32):
-            both = []
-            for k in (2 * i, 2 * i + 1):
-                near = jnp.broadcast_to(tile[:, k : k + 1], (8, 128))
-                later = jnp.broadcast_to(tile[:, k + 64 : k + 65], (8, 128))
-                both.append(jnp.where(col == 0, near, jnp.where(col == 1, later, 0.0)))
-            off[source, pl.ds(i * 16, 16), :] = jnp.concatenate(both, axis=0).astype(BF16)
+        q = qin[source].astype(F32) * (HD**-0.5 * LOG2E)
+        high = q.astype(BF16)
+        qa[source] = jnp.concatenate([high, ones, (q - high.astype(F32)).astype(BF16), zero], axis=0)
         for core in (0, 1):
             pl.when(c == core)(lambda core=core: pass_on(1 - core, source).wait_recv())
+        tile = min_[source] * LOG2E
+        for i in range(32):
+            packed = kin[source, pl.ds(i * 16, 16), :].astype(F32)
+            for first in (0, 64):
+                both = []
+                for k in (0, 1):
+                    at = first + 2 * i + k
+                    value = jnp.broadcast_to(tile[:, at : at + 1], (8, 128))
+                    top = value.astype(BF16).astype(F32)
+                    key = packed[8 * k : 8 * k + 8]
+                    key = pltpu.roll(key, 64, 1) if first else key
+                    extra = jnp.where(col == HD, top, jnp.where(col == HD + 1, value - top, 0.0))
+                    both.append(jnp.where(col < HD, key, extra))
+                keys_in[source, pl.ds(first * 8 + i * 16, 16), :] = jnp.concatenate(both, axis=0).astype(BF16)
 
     def where_is(u):
         one, two = lax.rem(z + nth(u[0]), 8), lax.rem(z + nth(u[1]), 8)
@@ -414,17 +446,19 @@
         ends = k == n
         return (jnp.where(ends, n + 1, n), jnp.where(ends, 0, k + 1))
 
-    def scores(u, s_ref):
+    def ready(u):
         pl.when(jnp.logical_and(u[1] == 0, u[0] < NZ))(lambda: arrive(u[0]))
+
+    def scores(u, e_ref, r_ref, t_ref):
         zq, zk = where_is((jnp.minimum(u[0], NZ - 1), u[1]))
-        lhs = jnp.concatenate([kin[zk], off[zk]], axis=1)
-        s_ref[0:512, :] = jnp.dot(lhs, qa[zq], preferred_element_type=F32)
-        s_ref[512:1024, :] = jnp.dot(lhs, qb[zq], preferred_element_type=F32)
-
-    def weights(u, s_ref, w_ref):
+        keys_ = keys_in[zk]
+        score = jnp.dot(jnp.concatenate([keys_, keys_], axis=1), qa[zq], preferred_element_type=F32)
+        which = jnp.where(zq == zk, 1 + lax.rem(zq, 2), 0)
+        keep(score, cap.at[which], e_ref, r_ref, t_ref)
+
+    def weights_of(u, e_ref, r_ref, t_ref, w_ref):
         zq, zk = where_is(u)
-        which = jnp.where(zq == zk, 1 + lax.rem(zq, 2), 0)
-        weigh(s_ref, cap.at[which], r_ref, w_ref, left.at[zq * NZ + zk])
+        weigh(e_ref, r_ref, t_ref, w_ref, left.at[zq * NZ + zk])
 
     def values(u, w_ref):
         zq, zk = where_is(u)
@@ -432,19 +466,22 @@
 
     start = jnp.int32(0)
     w1[...] = jnp.zeros_like(w1)
-    scores((start, start), s0)
-
+    share(start)
+    ready((start, start))
+    scores((start, start), e0, r0, t0)
     remote(stat, stat_in, ss.at[0], sr.at[0], tp=1 - c).start()
 
     def pair(_, state):
         before, now = state
         after = following(now)
-        scores(after, s1)
-        weights(now, s0, w0)
+        last = following(after)
+        ready(after)
+        ready(last)
+        scores(after, e1, r1, t1)
+        weights_of(now, e0, r0, t0, w0)
         values(before, w1)
-        last = following(after)
-        scores(last, s0)
-        weights(after, s1, w1)
+        scores(last, e0, r0, t0)
+        weights_of(after, e1, r1, t1, w1)
         values(now, w0)
         return (after, last)
 
@@ -490,8 +527,9 @@
         own_part[f] = jnp.where(c == 0, low, high)
         part_out[f] = jnp.where(c == 0, high, low)
         theirs.append(remote(part_out.at[f], part_in.at[f], ps.at[f], pr.at[f], tp=1 - c))
-    for copy in theirs:
-        copy.start()
+        if f > 0:
+            theirs[f - 1].start()
+    theirs[3].start()
     for f, copy in enumerate(theirs):
         copy.wait()
         total = own_part[f].astype(F32) + part_in[f].astype(F32)
@@ -510,6 +548,7 @@
         def _(core=core):
             for source in range(NZ):
                 pass_on(core, source).wait_send()
+            hand_on(core).wait_send()
 
     ring_y.sent()
     ring_x.sent()
@@ -552,13 +591,15 @@
             vm((4, 128, 512), BF16),
             vm((4, 128, 512), BF16),
             vm((NZ, 256, QB), BF16),
-            vm((NZ, 256, QB), BF16),
-            vm((NZ, 512, 128), BF16),
+            vm((NZ, UNIT, 128), BF16),
             vm((UNIT, QB), F32),
             vm((UNIT, QB), F32),
             vm((UNIT, QB), BF16),
             vm((UNIT, QB), BF16),
             vm((256, QB), F32),
+            vm((256, QB), F32),
+            vm((8, QB), F32),
+            vm((8, QB), F32),
             vm((3, UNIT, QB), F32),
             vm((NZ * NZ, 8, QB), F32),
             vm((NZ * NZ, HD, QB), F32),
@@ -566,7 +607,7 @@
             vm((8, HD, QB), BF16),
         ]
         + sems(5, 6, 6, 6, 6, 4, 4, 3, 3)
-        + sems(2, 6, 6, 24, 8, 8, 8, 8, 8, 8, 3, 4, 1, 4, 1, 1, 8, 8, 4, 4),
+        + sems(2, 6, 6, 24, 8, 8, 8, 8, 8, 1, 3, 4, 1, 4, 1, 1, 8, 8, 4, 4),
         compiler_params=pltpu.CompilerParams(
             collective_id=1, has_side_effects=True, vmem_limit_bytes=63 * 2**20
         ),

time: 121 us -> 93.4 us (0.77)
  Pallas kernels: 117 us -> 90 us
    pallas_call x1, Pallas kernels: 117 us -> 90 us  [layer(): pl.pallas_call(layer_kernel, out_shape=jax.ShapeDtypeStruct((128, 2048),...]
where the time goes in v3:
time: 93.4 us; the launch traced here: 93.2 us
  Pallas kernels  90 us (96%)
  local copies, waits for them, and re-layouts  2.58 us (3%)
    pallas_call x1, Pallas kernels, layer(): pl.pallas_call(layer_kernel, out_shape=jax.ShapeDtypeStruct((128, 2048),...  90 us
    unnamed x3, local copies, waits for them, and re-layouts  2.57 us

profile of v3, /device:TPU:1, one launch (start us, length us, event | category | flops | bytes accessed | tf_op | source)
XLA Modules:
  0.0 93.2 jit_solution(7302186155487370369)
XLA Ops:
  0.0 0.0 copy-start
  0.0 0.7 copy-done
  0.7 0.6 pad_convert_fusion.offx
  1.3 90.0 %layer.1 = bf16[128,2048]{1,0:T(8,128)(2,1)} custom-call(bf16[128,2048]{1,0:T(8,128)(2,1)} %bitcast.6, f32[1,2048]{1,0:T(1,128)} %bitcast.7, f32[4,2,8,128]{3,2,1,0:T(8,128)} %pad_convert_fusion.offx, f32[31,512]{1,0:T(8,128)} %taps.1, f32[1,512]{1,0:T(1,128)} %bitcast.9, bf16[512,512]{1,0:T(8,128)(2,1)} %wq.1, bf16[512,512]{1,0:T(8,128)(2,1)} %wk.1, ...), custom_call_target="tpu_custom_call" | custom-call | tf_op jit(solution)/shard_map/layer/pallas_call | solution.py:560
  91.3 1.9 %copy.14 = bf16[1,128,2048]{2,1,0:T(8,128)(2,1)} copy(bf16[1,128,2048]{2,1,0:T(8,128)(2,1)} %bitcast.5) | data formatting | bytes 1048576
  (1 shorter events, 0.0 us)
Async XLA Ops:
  0.0 0.7 copy-start

commit v4 on v3

--- a/solution.py
+++ b/solution.py
@@ -124,12 +124,12 @@
 
 
 def layer_kernel(
-    tok, tok_gain, offx, taps, gain, wq, wk, wv, wcv, wcg, wa, wc, out_ref,
+    tok, tok_gain, offx, taps, gain, wq, wk, wv, wcv, wcg, wa, wc, own_part, part_in,
     rows, weights, offs, full, kf, vf, vp, qt, kp, vt, m, gated,
-    kin, vin, qin, min_, gin, wout, ext, csum, stat, stat_in, hidden, heads, own_part, part_out, part_in,
+    kin, vin, qin, min_, gin, wout, ext, csum, stat, stat_in, hidden, heads, own_out, part_out, conv_part,
     qa, keys_in, e0, e1, w0, w1, r0, r1, t0, t1, cap, left, acc, oout, oin,
     ws, cxs, cxr, cys, cyr, cds, cdr, cos, cor,
-    wl, ys, yr, zs, ks, vs, qs, ms, ds, fs, xs, xr, hs, hr, ss, sr, os_, or_, ps, pr,
+    wl, ys, yr, zs, ks, vs, qs, ms, ds, fs, xs, xr, hs, hr, ss, sr, os_, or_, ps, pr, po,
 ):
     z, x, y, c = (lax.axis_index(n) for n in ("z", "x", "fs", "tp"))
     first_loads = [
@@ -189,8 +189,6 @@
         rows[x, c, at, :] = (floats * scale * tok_gain[...]).astype(BF16)
         return 0
 
-    lax.fori_loop(0, 8, norm, 0)
-    offs[x] = offx[x]
     for load in first_loads:
         load.wait()
     pl.semaphore_wait(
@@ -207,6 +205,8 @@
 
     across = [over(x, 0), over(ring_x.left, 1), over(ring_x.right, 2), over(lax.rem(x + 2, 4), 3)]
     ring_w.start()
+    lax.fori_loop(0, 8, norm, 0, unroll=4)
+    offs[x] = offx[x]
     ring_x.start()
     across[0].start()
     small = [
@@ -464,6 +464,25 @@
         zq, zk = where_is(u)
         acc[zq * NZ + zk] = jnp.dot(vin[zk], w_ref[...], preferred_element_type=F32)
 
+    def combine(zq):
+        total = acc[zq * NZ + zq].reshape(8, 8, QB)
+        rest = left[zq * NZ + zq]
+        for zk in range(zq - 1, -1, -1):
+            total = total + acc[zq * NZ + zk].reshape(8, 8, QB) * rest[None]
+            if zk > 0:
+                rest = rest * left[zq * NZ + zk]
+        oout[zq] = total.reshape(HD, QB).astype(BF16)
+
+    across_z = lax.rem(z + 4, 8)
+
+    def give(when):
+        for zq in range(NZ):
+            pl.when(when(zq))(lambda zq=zq: combine(zq))
+        for self_, copy, zq in backs:
+            pl.when(jnp.logical_and(other(self_), when(zq)))(copy.start)
+            own = local(oout.at[zq], oin.at[head], or_.at[head])
+            pl.when(jnp.logical_and(self_, when(zq)))(own.start)
+
     start = jnp.int32(0)
     w1[...] = jnp.zeros_like(w1)
     share(start)
@@ -471,8 +490,9 @@
     scores((start, start), e0, r0, t0)
     remote(stat, stat_in, ss.at[0], sr.at[0], tp=1 - c).start()
 
-    def pair(_, state):
+    def pair(p, state):
         before, now = state
+        pl.when(p == NZ * NZ // 4 - 1)(lambda: give(lambda zq: zq < across_z))
         after = following(now)
         last = following(after)
         ready(after)
@@ -487,18 +507,7 @@
 
     last, _ = lax.fori_loop(0, NZ * (NZ + 1) // 4, pair, ((start, start), (start, start)))
     values(last, w1)
-
-    for zq in range(NZ):
-        total = acc[zq * NZ + zq].reshape(8, 8, QB)
-        rest = left[zq * NZ + zq]
-        for zk in range(zq - 1, -1, -1):
-            total = total + acc[zq * NZ + zk].reshape(8, 8, QB) * rest[None]
-            if zk > 0:
-                rest = rest * left[zq * NZ + zk]
-        oout[zq] = total.reshape(HD, QB).astype(BF16)
-    for self_, copy, zq in backs:
-        pl.when(other(self_))(copy.start)
-        pl.when(self_)(local(oout.at[zq], oin.at[head], or_.at[head]).start)
+    give(lambda zq: zq >= across_z)
 
     remote(stat, stat_in, ss.at[0], sr.at[0], tp=1 - c).wait()
 
@@ -516,24 +525,28 @@
     lax.fori_loop(0, 8, finish, 0)
     ring_y.neighbours()
     ring_y.far()
+    for f in range(4):
+        conv_part[:, pl.ds(f * 512, 512)] = jnp.dot(hidden[...], wout[f, 1], preferred_element_type=F32)
     for h in range(8):
         local(oout.at[0], oin.at[h], or_.at[h]).wait()
     heads[...] = oin[...].reshape(512, QB).astype(F32).T.astype(BF16)
-    theirs = []
+    theirs, ours = [], []
     for f in range(4):
+        cols = pl.ds(f * 512, 512)
         total = jnp.dot(heads[...], wout[f, 0], preferred_element_type=F32)
-        total = (total + jnp.dot(hidden[...], wout[f, 1], preferred_element_type=F32)).astype(BF16)
+        total = (total + conv_part[:, cols]).astype(BF16)
         low, high = total[:128], total[128:]
-        own_part[f] = jnp.where(c == 0, low, high)
-        part_out[f] = jnp.where(c == 0, high, low)
-        theirs.append(remote(part_out.at[f], part_in.at[f], ps.at[f], pr.at[f], tp=1 - c))
+        own_out[:, cols] = jnp.where(c == 0, low, high)
+        part_out[:, cols] = jnp.where(c == 0, high, low)
+        theirs.append(remote(part_out.at[:, cols], part_in.at[:, cols], ps.at[f], pr.at[f], tp=1 - c))
+        ours.append(local(own_out.at[:, cols], own_part.at[:, cols], po.at[f]))
         if f > 0:
             theirs[f - 1].start()
+            ours[f - 1].start()
     theirs[3].start()
-    for f, copy in enumerate(theirs):
+    ours[3].start()
+    for copy in theirs + ours:
         copy.wait()
-        total = own_part[f].astype(F32) + part_in[f].astype(F32)
-        out_ref[:, pl.ds(f * 512, 512)] = total.astype(BF16)
 
     for cond, copy in sends:
         pl.when(cond)(copy.wait_send)
@@ -559,9 +572,9 @@
     vm = pltpu.VMEM
     return pl.pallas_call(
         layer_kernel,
-        out_shape=jax.ShapeDtypeStruct((128, 2048), BF16),
+        out_shape=(jax.ShapeDtypeStruct((128, 2048), BF16),) * 2,
         in_specs=[VM] * 5 + [HBM] * 7,
-        out_specs=VM,
+        out_specs=(HBM, HBM),
         scratch_shapes=[
             vm((NX, 2, 128, 2048), BF16),
             vm((4, 512, 640), BF16),
@@ -587,9 +600,9 @@
             vm((2, 256, 128), F32),
             vm((256, 512), BF16),
             vm((256, 512), BF16),
-            vm((4, 128, 512), BF16),
-            vm((4, 128, 512), BF16),
-            vm((4, 128, 512), BF16),
+            vm((128, 2048), BF16),
+            vm((128, 2048), BF16),
+            vm((256, 2048), F32),
             vm((NZ, 256, QB), BF16),
             vm((NZ, UNIT, 128), BF16),
             vm((UNIT, QB), F32),
@@ -607,7 +620,7 @@
             vm((8, HD, QB), BF16),
         ]
         + sems(5, 6, 6, 6, 6, 4, 4, 3, 3)
-        + sems(2, 6, 6, 24, 8, 8, 8, 8, 8, 1, 3, 4, 1, 4, 1, 1, 8, 8, 4, 4),
+        + sems(2, 6, 6, 24, 8, 8, 8, 8, 8, 1, 3, 4, 1, 4, 1, 1, 8, 8, 4, 4, 4),
         compiler_params=pltpu.CompilerParams(
             collective_id=1, has_side_effects=True, vmem_limit_bytes=63 * 2**20
         ),
@@ -621,10 +634,11 @@
 ):
     tile = key_offset.astype(F32).T.reshape(NX, 2, 2, 128)
     tile = jnp.pad(tile, ((0, 0), (0, 0), (0, 6), (0, 0)))
-    return layer(
+    own, other = layer(
         tokens[0], norm_gain[None], tile, conv_kernel, conv_gain[None],
         w_query, w_key, w_value, w_conv_value, w_conv_gate, w_attn_out, w_conv_out,
-    )[None]
+    )
+    return (own.astype(F32) + other.astype(F32)).astype(BF16)[None]
 
 
 def solution(mesh):

time: 93.4 us -> 91.3 us (0.978)
  Pallas kernels: 90 us -> 87.6 us
  other arithmetic: 0.62 us -> 2.74 us
  local copies, waits for them, and re-layouts: 2.58 us -> 0.7 us
    pallas_call x1, Pallas kernels: 90 us -> 87.6 us  [layer(): pl.pallas_call(layer_kernel, out_shape=(jax.ShapeDtypeStruct((128, 2048),...]
    broadcast_in_dim x0 -> x1, other arithmetic: none -> 2.12 us  [shards(): return (own.astype(F32) + other.astype(F32)).astype(BF16)[None]]
    unnamed x3 -> x2, local copies, waits for them, and re-layouts: 2.57 us -> 0.69 us
where the time goes in v4:
time: 91.3 us; the launch traced here: 91 us
  Pallas kernels  87.6 us (96%)
  other arithmetic  2.74 us (3%)
    pallas_call x1, Pallas kernels, layer(): pl.pallas_call(layer_kernel, out_shape=(jax.ShapeDtypeStruct((128, 2048),...  87.6 us
    broadcast_in_dim x1, other arithmetic, shards(): return (own.astype(F32) + other.astype(F32)).astype(BF16)[None]  2.12 us

profile of v4, /device:TPU:1, one launch (start us, length us, event | category | flops | bytes accessed | tf_op | source)
XLA Modules:
  0.0 91.0 jit_solution(1531671165207832776)
XLA Ops:
  0.0 0.0 copy-start
  0.0 0.7 copy-done
  0.7 0.6 pad_convert_fusion.offx
  1.3 87.6 %layer.1 = (bf16[128,2048]{1,0:T(8,128)(2,1)}, bf16[128,2048]{1,0:T(8,128)(2,1)}) custom-call(bf16[128,2048]{1,0:T(8,128)(2,1)} %bitcast.6, f32[1,2048]{1,0:T(1,128)} %bitcast.7, f32[4,2,8,128]{3,2,1,0:T(8,128)} %pad_convert_fusion.offx, f32[31,512]{1,0:T(8,128)} %taps.1, f32[1,512]{1,0:T(1,128)} %bitcast.9, bf16[512,512]{1,0:T(8,128)(2,1)} %wq.1, ...), custom_call_target="tpu_custom_call" | custom-call | tf_op jit(solution)/shard_map/layer/pallas_call | solution.py:573
  88.9 2.1 %fusion = bf16[1,128,2048]{2,1,0:T(8,128)(2,1)} fusion(bf16[128,2048]{1,0:T(8,128)(2,1)} %get-tuple-element.8, bf16[128,2048]{1,0:T(8,128)(2,1)} %get-tuple-element.7), kind=kLoop, calls=%fused_computation.1 | loop fusion | flops 1048576 | bytes 1572864 | tf_op jit(solution)/shard_map/broadcast_in_dim | solution.py:641
  (1 shorter events, 0.0 us)
Async XLA Ops:
  0.0 0.7 copy-start

commit v5 on v4

--- a/solution.py
+++ b/solution.py
@@ -139,7 +139,7 @@
         for i, w in enumerate((wq, wk, wv, wcv, wcg))
     ]
     loads = [pltpu.make_async_copy(w, wout.at[y, i], wl.at[i]) for i, w in enumerate((wa, wc))]
-    for load in first_loads + loads:
+    for load in first_loads:
         load.start()
     home = z // 4
     here = home == c
@@ -209,6 +209,8 @@
     offs[x] = offx[x]
     ring_x.start()
     across[0].start()
+    for load in loads:
+        load.start()
     small = [
         remote(offx.at[lax.rem(x + d, 4)], offs.at[x], cos.at[d - 1], cor.at[d - 1], x=lax.rem(x + d, 4))
         for d in (1, 2, 3)

time: 91.3 us -> 91.3 us (level)
  no operation moved by 1% of the time
where the time goes in v5:
time: 91.3 us; the launch traced here: 91.1 us
  Pallas kernels  87.7 us (96%)
  other arithmetic  2.74 us (3%)
    pallas_call x1, Pallas kernels, layer(): pl.pallas_call(layer_kernel, out_shape=(jax.ShapeDtypeStruct((128, 2048),...  87.7 us
    broadcast_in_dim x1, other arithmetic, shards(): return (own.astype(F32) + other.astype(F32)).astype(BF16)[None]  2.12 us

profile of v5, /device:TPU:1, one launch (start us, length us, event | category | flops | bytes accessed | tf_op | source)
XLA Modules:
  0.0 91.1 jit_solution(7757220967412051801)
XLA Ops:
  0.0 0.0 copy-start
  0.0 0.7 copy-done
  0.7 0.6 pad_convert_fusion.offx
  1.3 87.7 %layer.1 = (bf16[128,2048]{1,0:T(8,128)(2,1)}, bf16[128,2048]{1,0:T(8,128)(2,1)}) custom-call(bf16[128,2048]{1,0:T(8,128)(2,1)} %bitcast.6, f32[1,2048]{1,0:T(1,128)} %bitcast.7, f32[4,2,8,128]{3,2,1,0:T(8,128)} %pad_convert_fusion.offx, f32[31,512]{1,0:T(8,128)} %taps.1, f32[1,512]{1,0:T(1,128)} %bitcast.9, bf16[512,512]{1,0:T(8,128)(2,1)} %wq.1, ...), custom_call_target="tpu_custom_call" | custom-call | tf_op jit(solution)/shard_map/layer/pallas_call | solution.py:575
  89.0 2.1 %fusion = bf16[1,128,2048]{2,1,0:T(8,128)(2,1)} fusion(bf16[128,2048]{1,0:T(8,128)(2,1)} %get-tuple-element.8, bf16[128,2048]{1,0:T(8,128)(2,1)} %get-tuple-element.7), kind=kLoop, calls=%fused_computation.1 | loop fusion | flops 1048576 | bytes 1572864 | tf_op jit(solution)/shard_map/broadcast_in_dim | solution.py:643
  (1 shorter events, 0.0 us)
Async XLA Ops:
  0.0 0.7 copy-start
